TPU v7x, 128 devices: a whole 4x4x4 slice. The times are simulated.
128 devices in a mesh: dp: 4 (over x), kv: 16 (over z, y), tp: 2 (over core).
Axes of the slice: x: 4, y: 4, z: 4, core: 2. Of those that a mesh axis runs over, the one named last changes fastest.
Arguments:
- tokens: bfloat16 [32, 2048], P('dp', ('kv', 'tp')), may hold values from -30 to 30
- attention_gain: bfloat16 [2048], P(('kv', 'tp')), may hold values from 0.099609375 to 1.8984375
- query_one: bfloat16 [2048, 512], P('kv', 'tp'), may hold values from -0.125 to 0.125
- query_two: bfloat16 [2048, 512], P('kv', 'tp'), may hold values from -0.125 to 0.125
- key_one: bfloat16 [2048, 512], P('kv', 'tp'), may hold values from -2 to 2
- key_two: bfloat16 [2048, 512], P('kv', 'tp'), may hold values from -2 to 2
- value_weight: bfloat16 [2048, 1024], P('kv', 'tp'), may hold values from -0.125 to 0.125
- head_second_weight: float32 [8], P('tp'), may hold values from 0.3 to 0.8
- head_gain: float32 [128], replicated, may hold values from 0.1 to 1.9
- out_weight: bfloat16 [1024, 2048], P('tp', 'kv'), may hold values from -0.375 to 0.375
- mixer_gain: bfloat16 [2048], P(('kv', 'tp')), may hold values from 0.099609375 to 1.8984375
- gate_weight: bfloat16 [2048, 5632], P('kv', 'tp'), may hold values from -0.125 to 0.125
- up_weight: bfloat16 [2048, 5632], P('kv', 'tp'), may hold values from -0.125 to 0.125
- down_weight: bfloat16 [5632, 2048], P('tp', 'kv'), may hold values from -0.15625 to 0.15625
- key_cache: bfloat16 [32, 16384, 8, 128], P('dp', 'kv', 'tp'), may hold values from -240 to 240
- value_cache: bfloat16 [32, 16384, 8, 128], P('dp', 'kv', 'tp'), may hold values from -6 to 6
Outputs:
- layer_out: bfloat16 [32, 2048], P('dp', ('kv', 'tp'))
All inputs are finite; a program needn't handle non-finite values.
Results may differ from a plain program's by a relative error of at most 0.02.
Values may be sent and summed in bfloat16 or wider, within the bound.
A program may use at most 64 MiB of HBM per device.

v0:
```python
import jax
import jax.numpy as jnp
from jax import lax
from jax.sharding import Mesh
from jax.sharding import PartitionSpec as P

DH = 64
KV = ("kv_0", "kv_1")
KV_TP = ("kv_0", "kv_1", "tp")


NORM_EPSILON = 1e-06
HEAD_EPSILON = 1e-05
HEAD_SCALE = 0.8
ROTARY_BASE = 10000.0


def turned_gather(arrays, axis, dims):
    turned = [jnp.moveaxis(a, dim, 0) for a, dim in zip(arrays, dims)]
    both = jnp.concatenate([t.reshape(len(t), -1) for t in turned], axis=1)
    filled, at, done = (lax.all_gather(both, axis, axis=0, tiled=True), 0, [])
    for t, dim in zip(turned, dims):
        piece = filled[:, at : at + t[0].size].reshape(-1, *t.shape[1:])
        done.append(jnp.moveaxis(piece, 0, dim))
        at += t[0].size
    return tuple(done)


def copy_for_each(value, axis):
    copies = jnp.broadcast_to(value, (lax.axis_size(axis), *value.shape))
    return lax.all_to_all(copies, axis, split_axis=0, concat_axis=0, tiled=True)


def of_everyone(value, axis):
    everything = copy_for_each(value, axis)
    return jnp.sum(everything, axis=0)


def in_one(arrays, axis):
    line, at, done = (jnp.concatenate([a.reshape(-1) for a in arrays]), 0, [])
    subtotal = of_everyone(line, axis)
    for a in arrays:
        done.append(subtotal[at : at + a.size].reshape(a.shape))
        at += a.size
    return tuple(done)


def collected_together(value, axis):
    leaves = jax.tree.leaves(value)
    turns = sorted(range(len(leaves)), key=lambda k: -leaves[k].size)
    width = (1, *leaves[turns[0]].shape)[-1]
    lines = [
        jnp.pad(leaves[k].reshape(-1), (0, -leaves[k].size % width)).reshape(-1, width)
        for k in turns
    ]
    both, at, found = (lax.all_gather(jnp.concatenate(lines), axis), 0, {})
    for k, line in zip(turns, lines):
        piece = both[:, at : at + len(line)].reshape(len(both), -1)
        found[k] = piece[:, : leaves[k].size].reshape(-1, *leaves[k].shape)
        at += len(line)
    numbers = iter(range(len(leaves)))
    return jax.tree.map(lambda _: found[next(numbers)], value)


def joined_all(value, axes, combine):
    for axis in axes:
        pieces = collected_together(value, axis)
        value = jax.tree.map(lambda part: part[0], pieces)
        for k in range(1, lax.axis_size(axis)):
            value = combine(value, jax.tree.map(lambda part: part[k], pieces))
    return value


def split_up(value, dim, devices):
    before, after = (value.shape[:dim], value.shape[dim + 1 :])
    return jnp.moveaxis(value.reshape(*before, devices, -1, *after), dim, 0)


def sent_and_summed(value, axis, dim):
    parts = split_up(value, dim, lax.axis_size(axis))
    arrived = lax.all_to_all(parts, axis, split_axis=0, concat_axis=0, tiled=True)
    return arrived.astype(jnp.float32).sum(axis=0)


def sent_and_summed_2(value, axis, dim):
    devices = lax.axis_size(axis)
    parts = lax.all_to_all(split_up(value, dim, devices), axis, 0, 0, tiled=True)
    return jnp.sum(parts, axis=0)


def in_one_piece(arrays, axis, dim, along):
    both = jnp.concatenate(arrays, axis=along)
    filled, at, done = (sent_and_summed_2(both, axis, dim), 0, [])
    for a in arrays:
        done.append(lax.slice_in_dim(filled, at, at + a.shape[along], axis=along))
        at += a.shape[along]
    return tuple(done)


def laid_out(parts, dim):
    shape = list(parts.shape[1:])
    shape[dim] *= parts.shape[0]
    return jnp.moveaxis(parts, 0, dim).reshape(shape)


def gathered_copies(value, axis, dim):
    parts = copy_for_each(value, axis)
    return laid_out(parts, dim)


def rotate(vectors, position):
    half_width = vectors.shape[-1] // 2
    frequency = 1.0 / ROTARY_BASE ** (jnp.arange(half_width, dtype=jnp.float32) / half_width)
    angles = position * frequency
    cosine = jnp.cos(angles)
    sine_value = jnp.sin(angles)
    lead_half = vectors[..., :half_width]
    tail_half = vectors[..., half_width:]
    return jnp.concatenate(
        [lead_half * cosine - tail_half * sine_value, tail_half * cosine + lead_half * sine_value],
        axis=-1,
    )


def combine(earlier, later):
    peak_left, total_left, weighted_left = earlier
    peak_right, total_right, weighted_right = later
    peak_score = jnp.maximum(peak_left, peak_right)
    factor_left = jnp.exp(peak_left - peak_score)
    factor_right = jnp.exp(peak_right - peak_score)
    return (
        peak_score,
        total_left * factor_left + total_right * factor_right,
        weighted_left * factor_left[..., None] + weighted_right * factor_right[..., None],
    )


def shards(
    tokens,
    attention_gain,
    query_one,
    query_two,
    key_one,
    key_two,
    value_weight,
    head_second_weight,
    head_gain,
    out_weight,
    mixer_gain,
    gate_weight,
    up_weight,
    down_weight,
    key_cache,
    value_cache,
):
    row_count = tokens.shape[0]
    position_group = lax.axis_size(KV)
    model_width = tokens.shape[1] * position_group * lax.axis_size("tp")
    local_heads = query_one.shape[1] // DH
    local_positions = key_cache.shape[1]
    position = jnp.float32(local_positions * position_group)
    score_scale = DH ** (-0.5)
    token_values = tokens.astype(jnp.float32)
    row_block, gain_block = turned_gather((tokens, attention_gain), "tp", (1, 0))
    block_values = row_block.astype(jnp.float32)
    scaled = (block_values * gain_block.astype(jnp.float32)).astype(jnp.bfloat16)
    query_first = jnp.dot(scaled, query_one, preferred_element_type=jnp.float32)
    query_second = jnp.dot(scaled, query_two, preferred_element_type=jnp.float32)
    key_first = jnp.dot(scaled, key_one, preferred_element_type=jnp.float32)
    key_second = jnp.dot(scaled, key_two, preferred_element_type=jnp.float32)
    value_part = jnp.dot(scaled, value_weight, preferred_element_type=jnp.float32)
    block_square = jnp.sum(block_values * block_values, axis=1)
    query_first, query_second, key_first, key_second, value_part, square_total = in_one(
        (query_first, query_second, key_first, key_second, value_part, block_square), KV
    )
    row_ratio = lax.rsqrt(square_total / model_width + NORM_EPSILON)[:, None]

    def paired(lead_part, tail_part):
        both = jnp.stack(
            [
                (lead_part * row_ratio).reshape(row_count, local_heads, DH),
                (tail_part * row_ratio).reshape(row_count, local_heads, DH),
            ],
            axis=2,
        )
        return rotate(both, position).astype(jnp.bfloat16)

    queries = paired(query_first, query_second)
    new_keys = paired(key_first, key_second)
    new_values = (
        (value_part * row_ratio).astype(jnp.bfloat16).reshape(row_count, local_heads, 2 * DH)
    )
    zero_half = jnp.zeros((row_count, local_heads, DH), jnp.bfloat16)
    padded_query_rows = jnp.stack(
        [
            jnp.concatenate([queries[:, :, 0], zero_half], axis=-1),
            jnp.concatenate([zero_half, queries[:, :, 1]], axis=-1),
        ],
        axis=2,
    )
    logit_scores = (
        jnp.einsum(
            "bhmk,bphk->bhmp", padded_query_rows, key_cache, preferred_element_type=jnp.float32
        )
        * score_scale
    )
    peak_score = jnp.max(logit_scores, axis=-1)
    exponent = jnp.exp(logit_scores - peak_score[..., None])
    weight_sum = jnp.sum(exponent, axis=-1)
    weighted = jnp.einsum(
        "bhmp,bphe->bhme",
        exponent.astype(jnp.bfloat16),
        value_cache,
        preferred_element_type=jnp.float32,
    )
    peak_score, weight_sum, weighted = joined_all((peak_score, weight_sum, weighted), KV, combine)
    own_score = (
        jnp.sum(queries.astype(jnp.float32) * new_keys.astype(jnp.float32), axis=-1) * score_scale
    )
    final_peak = jnp.maximum(peak_score, own_score)
    cache_factor = jnp.exp(peak_score - final_peak)
    own_weight = jnp.exp(own_score - final_peak)
    weight_sum = weight_sum * cache_factor + own_weight
    weighted = (
        weighted * cache_factor[..., None]
        + own_weight[..., None] * new_values.astype(jnp.float32)[:, :, None, :]
    )
    averaged = weighted / weight_sum[..., None]
    difference = averaged[:, :, 0] - head_second_weight[None, :, None] * averaged[:, :, 1]
    inverse_norm = lax.rsqrt(
        jnp.mean(difference * difference, axis=-1, keepdims=True) + HEAD_EPSILON
    )
    attended = (difference * inverse_norm * head_gain[None, None, :] * HEAD_SCALE).astype(
        jnp.bfloat16
    )
    attended = attended.reshape(row_count, local_heads * 2 * DH)
    attention_term = jnp.dot(attended, out_weight, preferred_element_type=jnp.float32)
    attention_out = sent_and_summed(attention_term.astype(jnp.bfloat16), "tp", 1)
    mixed = (token_values + attention_out).astype(jnp.bfloat16)
    mixed_values = mixed.astype(jnp.float32)
    mixer_block, mixer_gain_block = turned_gather((mixed, mixer_gain), "tp", (1, 0))
    mixer_block_values = mixer_block.astype(jnp.float32)
    mixer_scaled = (mixer_block_values * mixer_gain_block.astype(jnp.float32)).astype(jnp.bfloat16)
    gate_part = jnp.dot(mixer_scaled, gate_weight, preferred_element_type=jnp.float32)
    up_part = jnp.dot(mixer_scaled, up_weight, preferred_element_type=jnp.float32)
    mixer_square = jnp.sum(mixer_block_values * mixer_block_values, axis=1)
    square_columns = jnp.broadcast_to(mixer_square[:, None], (row_count, position_group))
    gate_sum, up_sum, total_column = (
        *in_one_piece((gate_part, up_part), KV, 1, 0),
        sent_and_summed_2(square_columns, KV, 1),
    )
    mixer_total = total_column[:, 0]
    mixer_ratio = lax.rsqrt(mixer_total / model_width + NORM_EPSILON)[:, None]
    hidden_share = (jax.nn.silu(gate_sum * mixer_ratio) * (up_sum * mixer_ratio)).astype(
        jnp.bfloat16
    )
    hidden_state = gathered_copies(hidden_share, KV, 1)
    mixer_term = jnp.dot(hidden_state, down_weight, preferred_element_type=jnp.float32)
    mixer_out = sent_and_summed(mixer_term.astype(jnp.bfloat16), "tp", 1)
    return (mixed_values + mixer_out).astype(jnp.bfloat16)


def solution(mesh):
    torus = Mesh(
        mesh.devices.reshape(mesh.shape["dp"], 4, 4, mesh.shape["tp"]), ("dp", "kv_0", "kv_1", "tp")
    )
    return jax.shard_map(
        shards,
        mesh=torus,
        in_specs=(
            P("dp", KV_TP),
            P(KV_TP),
            P(KV, "tp"),
            P(KV, "tp"),
            P(KV, "tp"),
            P(KV, "tp"),
            P(KV, "tp"),
            P("tp"),
            P(),
            P("tp", KV),
            P(KV_TP),
            P(KV, "tp"),
            P(KV, "tp"),
            P("tp", KV),
            P("dp", KV, "tp", None),
            P("dp", KV, "tp", None),
        ),
        out_specs=P("dp", KV_TP),
        check_vma=False,
    )
```

profile of v0, /device:TPU:1, one launch (start us, length us, event | category | flops | bytes accessed | tf_op | source)
XLA Modules:
  0.0 119.3 jit_solution(6227983753720261710)
XLA Ops:
  0.0 0.8 maximum_bitcast_fusion.2
  0.8 2.8 %all-gather.2 = bf16[2,64,9]{1,2,0:T(8,128)(2,1)S(1)} all-gather(bf16[1,64,9]{1,2,0:T(8,128)(2,1)S(1)} %maximum_bitcast_fusion.2), channel_id=1, replica_groups=mesh['dp'=4,'kv_0'=4,'kv_1'=4,'tp'=2] {'tp'}, dimensions={0}, use_global_device_ids=true | all-gather | bytes 3456 | tf_op jit(solution)/shard_map/all_gather | solution.py:21
  3.6 0.1 reshape.579
  3.7 0.1 fusion.54
  3.8 1.0 convolution_bitcast_fusion.4
  4.8 1.0 convolution_bitcast_fusion.3
  5.8 1.0 convolution_bitcast_fusion.2
  6.8 1.0 convolution_bitcast_fusion.1
  7.8 1.0 convolution_bitcast_fusion
  8.8 1.3 %broadcast_in_dim.4 = f32[16,1,12296]{2,1,0:T(1,128)} broadcast(f32[12296]{0:T(1024)S(1)} %constant_dynamic-update-slice_fusion), dimensions={2} | broadcast | bytes 836128 | tf_op jit(solution)/shard_map/broadcast_in_dim | solution.py:30
  10.1 7.9 %all-to-all-start = ((f32[16,1,12296]{2,1,0:T(1,128)}), f32[16,1,12296]{2,1,0:T(1,128)S(1)}, u32[]{:S(2)}, u32[]{:S(2)}) async-start(f32[16,1,12296]{2,1,0:T(1,128)} %broadcast_in_dim.4), calls=%async_computation | async-start | bytes 1589248 | tf_op jit(solution)/shard_map/all_to_all | solution.py:31
  18.1 0.7 broadcast_bitcast_fusion
  18.8 12.8 %all-to-all-done = f32[16,1,12296]{2,1,0:T(1,128)S(1)} async-done(((f32[16,1,12296]{2,1,0:T(1,128)}), f32[16,1,12296]{2,1,0:T(1,128)S(1)}, u32[]{:S(2)}, u32[]{:S(2)}) %all-to-all-start) | async-done | bytes 786976 | tf_op jit(solution)/shard_map/all_to_all | solution.py:31
  31.7 0.5 reduce_sum.91
  32.6 0.1 subtract_convert_fusion
  32.7 0.1 fusion.40
  32.9 5.7 %fusion.94 = (f32[8,4,2]{2,1,0:T(4,128)S(1)}, f32[8,4,2,1024]{3,2,1,0:T(2,128)S(1)}) fusion(bf16[8,1024,4,128]{3,2,1,0:T(4,128)(2,1)} %param.30, bf16[8,4,1,128]{3,2,1,0:T(2,128)(2,1)S(1)} %copy.107, bf16[8,4,1,128]{3,2,1,0:T(2,128)(2,1)S(1)} %copy.106), kind=kOutput, calls=%fused_computation.184 | convolution fusion | flops 16940992 | bytes 8667392 | tf_op jit(solution)/shard_map/bhmk,bphk->bhmp/dot_general | solution.py:202
  38.7 0.1 reshape.556
  38.8 0.3 fusion.7
  39.2 4.9 %fusion = f32[8,4,2,128]{3,2,1,0:T(2,128)S(1)} fusion(bf16[8,1024,4,128]{3,2,1,0:T(4,128)(2,1)} %param.31, f32[8,4,2,1024]{3,2,1,0:T(2,128)S(1)} %get-tuple-element.57, f32[8,4,2]{2,1,0:T(4,128)S(1)} %get-tuple-element.56), kind=kOutput, calls=%fused_computation | convolution fusion | flops 16908288 | bytes 8683776 | tf_op jit(solution)/shard_map/bhmp,bphe->bhme/dot_general | solution.py:210
  44.1 0.1 reshape.558
  44.3 9.6 %all-gather.3 = f32[4,66,128]{2,1,0:T(8,128)S(1)} all-gather(f32[1,66,128]{2,1,0:T(8,128)S(1)} %maximum_bitcast_fusion), channel_id=2, replica_groups=mesh['dp'=4,'kv_0'=4,'kv_1'=4,'tp'=2] {'kv_0'}, dimensions={0}, use_global_device_ids=true | all-gather | bytes 168960 | tf_op jit(solution)/shard_map/all_gather | solution.py:56
  53.9 0.1 fusion.12
  54.0 9.6 %all-gather.4 = f32[4,66,128]{2,1,0:T(8,128)S(1)} all-gather(f32[1,66,128]{2,1,0:T(8,128)S(1)} %maximum_bitcast_fusion.1), channel_id=3, replica_groups=mesh['dp'=4,'kv_0'=4,'kv_1'=4,'tp'=2] {'kv_1'}, dimensions={0}, use_global_device_ids=true | all-gather | bytes 168960 | tf_op jit(solution)/shard_map/all_gather | solution.py:56
  63.7 0.1 squeeze.105
  63.8 0.1 copy.111
  64.0 0.1 squeeze.104
  64.1 0.1 copy.112
  64.2 0.1 squeeze.107
  64.3 0.1 copy.116
  64.5 0.1 squeeze.109
  64.6 0.1 copy.119
  64.8 0.1 squeeze.111
  64.9 0.1 copy.122
  65.0 0.1 squeeze.112
  65.2 0.1 copy.123
  65.3 0.1 squeeze.113
  65.4 0.1 copy.124
  65.5 0.1 squeeze.114
  65.7 0.1 copy.125
  65.9 0.2 multiply_reduce_fusion
  66.1 0.2 fusion.23
  66.4 0.2 fusion.38
  66.6 0.2 convolution_convert_fusion.1
  66.9 0.1 reshape.630
  67.0 10.2 %all_to_all.31 = bf16[2,2,256]{2,1,0:T(2,128)(2,1)S(1)} all-to-all(bf16[2,2,256]{2,1,0:T(2,128)(2,1)S(1)} %reshape.630), channel_id=1, replica_groups=mesh['dp'=4,'kv_0'=4,'kv_1'=4,'tp'=2] {'tp'}, dimensions={0} | all-to-all | bytes 4096 | tf_op jit(solution)/shard_map/all_to_all | solution.py:81
  77.3 1.8 %all-gather.5 = bf16[2,64,9]{1,2,0:T(8,128)(2,1)S(1)} all-gather(bf16[1,64,9]{1,2,0:T(8,128)(2,1)S(1)} %maximum_bitcast_fusion.3), channel_id=1, replica_groups=mesh['dp'=4,'kv_0'=4,'kv_1'=4,'tp'=2] {'tp'}, dimensions={0}, use_global_device_ids=true | all-gather | bytes 3456 | tf_op jit(solution)/shard_map/all_gather | solution.py:21
  79.1 0.1 reshape.585
  79.2 0.1 fusion.56
  79.3 0.2 fusion.59
  79.5 0.2 fusion.57
  79.7 0.6 transpose.84
  80.3 3.5 %all-to-all-start.3 = ((f32[16,8,1]{1,2,0:T(1,128)}), f32[16,8,1]{1,2,0:T(1,128)S(1)}, u32[]{:S(2)}, u32[]{:S(2)}) async-start(f32[16,8,1]{1,2,0:T(1,128)} %transpose.84), calls=%async_computation.3 | async-start | bytes 16384 | tf_op jit(solution)/shard_map/all_to_all | solution.py:87
  83.9 0.2 reshape.571
  84.1 0.8 copy.191
  84.9 5.3 %all-to-all-done.3 = f32[16,8,1]{1,2,0:T(1,128)S(1)} async-done(((f32[16,8,1]{1,2,0:T(1,128)}), f32[16,8,1]{1,2,0:T(1,128)S(1)}, u32[]{:S(2)}, u32[]{:S(2)}) %all-to-all-start.3) | async-done | bytes 544 | tf_op jit(solution)/shard_map/all_to_all | solution.py:87
  90.3 3.5 %all-to-all-start.2 = ((f32[16,16,176]{2,1,0:T(8,128)}), f32[16,16,176]{2,1,0:T(8,128)S(1)}, u32[]{:S(2)}, u32[]{:S(2)}) async-start(f32[16,16,176]{2,1,0:T(8,128)} %bitcast.218), calls=%async_computation.2 | async-start | bytes 524288 | tf_op jit(solution)/shard_map/all_to_all | solution.py:87
  93.8 7.5 %all-to-all-done.2 = f32[16,16,176]{2,1,0:T(8,128)S(1)} async-done(((f32[16,16,176]{2,1,0:T(8,128)}), f32[16,16,176]{2,1,0:T(8,128)S(1)}, u32[]{:S(2)}, u32[]{:S(2)}) %all-to-all-start.2) | async-done | bytes 180256 | tf_op jit(solution)/shard_map/all_to_all | solution.py:87
  101.5 9.4 %all_to_all.32 = bf16[16,8,176]{2,1,0:T(8,128)(2,1)S(1)} all-to-all(bf16[16,8,176]{2,1,0:T(8,128)(2,1)S(1)} %broadcast_in_dim.5), channel_id=1, replica_groups=mesh['dp'=4,'kv_0'=4,'kv_1'=4,'tp'=2] {'kv_0','kv_1'}, dimensions={0} | all-to-all | bytes 90112 | tf_op jit(solution)/shard_map/all_to_all | solution.py:31
  110.9 0.1 reshape.572
  111.0 0.2 convolution_convert_fusion
  111.3 0.1 reshape.632
  111.4 7.3 %all_to_all.33 = bf16[2,2,256]{2,1,0:T(2,128)(2,1)S(1)} all-to-all(bf16[2,2,256]{2,1,0:T(2,128)(2,1)S(1)} %reshape.632), channel_id=1, replica_groups=mesh['dp'=4,'kv_0'=4,'kv_1'=4,'tp'=2] {'tp'}, dimensions={0} | all-to-all | bytes 4096 | tf_op jit(solution)/shard_map/all_to_all | solution.py:81
  118.8 0.6 add_convert_fusion.2
  (76 shorter events, 1.6 us)
Async XLA Ops:
  0.0 79.3 %copy-start = (bf16[128,2816]{1,0:T(8,128)(2,1)S(1)}, bf16[128,2816]{1,0:T(8,128)(2,1)}, u32[]{:S(2)}) copy-start(bf16[128,2816]{1,0:T(8,128)(2,1)} %param.27) | copy-start | bytes 2162692
  10.1 21.5 %all-to-all-start = ((f32[16,1,12296]{2,1,0:T(1,128)}), f32[16,1,12296]{2,1,0:T(1,128)S(1)}, u32[]{:S(2)}, u32[]{:S(2)}) async-start(f32[16,1,12296]{2,1,0:T(1,128)} %broadcast_in_dim.4), calls=%async_computation | async-start | bytes 1589248 | tf_op jit(solution)/shard_map/all_to_all | solution.py:31
  39.1 27.2 %copy-start.4 = (f32[4]{0:T(128)S(1)}, f32[4]{0:T(128)}, u32[]{:S(2)}) copy-start(f32[4]{0:T(128)} %param.23) | copy-start | bytes 52
  39.1 27.5 %copy-start.6 = (bf16[512,128]{1,0:T(8,128)(2,1)S(1)}, bf16[512,128]{1,0:T(8,128)(2,1)}, u32[]{:S(2)}) copy-start(bf16[512,128]{1,0:T(8,128)(2,1)} %param.25) | copy-start | bytes 393220
  39.2 38.1 %copy-start.3 = (bf16[8,64]{1,0:T(8,128)(2,1)S(1)}, bf16[8,64]{1,0:T(8,128)(2,1)}, u32[]{:S(2)}) copy-start(bf16[8,64]{1,0:T(8,128)(2,1)} %param.16) | copy-start | bytes 3076
  39.2 38.1 %copy-start.5 = (bf16[64]{0:T(256)(128)(2,1)S(1)}, bf16[64]{0:T(256)(128)(2,1)}, u32[]{:S(2)}) copy-start(bf16[64]{0:T(256)(128)(2,1)} %param.26) | copy-start | bytes 388
  39.2 40.3 %copy-start.1 = (bf16[128,2816]{1,0:T(8,128)(2,1)S(1)}, bf16[128,2816]{1,0:T(8,128)(2,1)}, u32[]{:S(2)}) copy-start(bf16[128,2816]{1,0:T(8,128)(2,1)} %param.28) | copy-start | bytes 2162692
  39.2 71.8 %copy-start.2 = (bf16[2816,128]{1,0:T(8,128)(2,1)S(1)}, bf16[2816,128]{1,0:T(8,128)(2,1)}, u32[]{:S(2)}) copy-start(bf16[2816,128]{1,0:T(8,128)(2,1)} %param.29) | copy-start | bytes 2162692
  80.3 9.9 %all-to-all-start.3 = ((f32[16,8,1]{1,2,0:T(1,128)}), f32[16,8,1]{1,2,0:T(1,128)S(1)}, u32[]{:S(2)}, u32[]{:S(2)}) async-start(f32[16,8,1]{1,2,0:T(1,128)} %transpose.84), calls=%async_computation.3 | async-start | bytes 16384 | tf_op jit(solution)/shard_map/all_to_all | solution.py:87
  90.3 11.1 %all-to-all-start.2 = ((f32[16,16,176]{2,1,0:T(8,128)}), f32[16,16,176]{2,1,0:T(8,128)S(1)}, u32[]{:S(2)}, u32[]{:S(2)}) async-start(f32[16,16,176]{2,1,0:T(8,128)} %bitcast.218), calls=%async_computation.2 | async-start | bytes 524288 | tf_op jit(solution)/shard_map/all_to_all | solution.py:87
where the time goes:
time: 120 us; the launch traced here: 119 us
  blocking collectives  50.7 us (42%)
  waiting for transfers between devices  25.7 us (21%)
  matrix products  16.4 us (14%)
  starting transfers between devices  14.9 us (12%)
  local copies, waits for them, and re-layouts  7.53 us (6%)
  other arithmetic  3.79 us (3%)
    all_gather x2, blocking collectives, collected_together(): both, at, found = (lax.all_gather(jnp.concatenate(lines), axis), 0, {})  19.2 us
    all_to_all x2, blocking collectives, sent_and_summed(): lax.all_to_all(parts, axis, split_axis=0, concat_axis=0, tiled=True)  17.4 us
    all_to_all x1, waiting for transfers between devices, copy_for_each(): return lax.all_to_all(copies, axis, split_axis=0, concat_axis=0, tiled=True)  12.8 us
    all_to_all x2, waiting for transfers between devices, sent_and_summed_2(): lax.all_to_all(split_up(value, dim, devices), axis, 0, 0, tiled=True)  12.8 us
    all_to_all x1, blocking collectives, copy_for_each(): return lax.all_to_all(copies, axis, split_axis=0, concat_axis=0, tiled=True)  9.4 us
    all_to_all x1, starting transfers between devices, copy_for_each(): return lax.all_to_all(copies, axis, split_axis=0, concat_axis=0, tiled=True)  7.88 us
    all_to_all x2, starting transfers between devices, sent_and_summed_2(): lax.all_to_all(split_up(value, dim, devices), axis, 0, 0, tiled=True)  7.01 us
    dot_general x1, matrix products, shards(): jnp.einsum('bhmk,bphk->bhmp', padded_query_rows, key_cache, preferred_ele...  5.74 us
  transfers between devices with their start and end apart: 3, of which 3 were waited for; matrix products, arithmetic and copies ran while one was open for 2% of the time, Pallas kernels for 0%

commit v1 on v0

v1 whole, which is shorter than its diff:
```python
import jax
import jax.numpy as jnp
import numpy as np
from jax import lax
from jax.experimental import pallas as pl
from jax.experimental.pallas import tpu as pltpu
from jax.sharding import PartitionSpec as P

MESH = pl.DeviceIdType.MESH
F32 = jnp.float32
BF16 = jnp.bfloat16

D = 2048
DH = 64
POSITIONS = 1024
HEADS = 4
ROWS = 8
KV = 16
FF = 2816
FT = FF // 128
HT = FT // 2
CACHE = KV * POSITIONS
NORM_EPSILON = 1e-06
HEAD_EPSILON = 1e-05
HEAD_SCALE = 0.8
FLOOR = -1e30
KEYS = POSITIONS * HEADS
QR = 33
CR = 72
GR = 24


def rotary_tables():
    half = DH // 2
    index = np.arange(half, dtype=np.float32) / np.float32(half)
    frequency = (np.float32(1.0) / np.power(np.float32(10000.0), index)).astype(np.float32)
    angle = (np.float32(CACHE) * frequency).astype(np.float32).astype(np.float64)
    cosine = np.tile(np.cos(angle).astype(np.float32), 4)
    sine = np.sin(angle).astype(np.float32)
    sine = np.tile(np.concatenate([-sine, sine]), 2)
    table = np.zeros((8, 128), np.float32)
    table[0], table[1] = cosine, sine
    return table


def layer_kernel(
    tok_h, ag_h, q1_h, q2_h, k1_h, k2_h, vw_h, hsw_h, hg_h, ow_h, mg_h, gw_h, uw_h, dw_h, kc_h, vc_h, tab_h,
    out_ref,
    tok_own, tok_far, ag_own, ag_far, mg_own, mg_far,
    q1_w, q2_w, k1_w, k2_w, vw_w, hsw, hg, ow_w, gw_w, uw_w, dw_w, kc, vc, tab,
    qx, ax, cx, gs, gx, hx, hs, qs, os_own, os_far, ds_own, ds_far,
    load_sem, pair_send, pair_recv, q_send, q_recv, a_send, a_recv, c_send, c_recv, g_send, g_recv, h_send, h_recv,
):
    dp, kv, tp = (lax.axis_index(a) for a in ("dp", "kv", "tp"))
    barrier = pltpu.get_barrier_semaphore()
    partner = (dp, kv, 1 - tp)
    peers = [lax.rem(kv + d, KV) for d in range(1, KV)]
    for p in peers:
        pl.semaphore_signal(barrier, 1, device_id=(dp, p, tp), device_id_type=MESH)
    pl.semaphore_signal(barrier, 1, device_id=partner, device_id_type=MESH)

    loads = []

    def load(src, dst):
        copy = pltpu.make_async_copy(src, dst, load_sem.at[len(loads)])
        copy.start()
        loads.append(copy)
        return copy

    first = [load(a, b) for a, b in ((tok_h, tok_own), (ag_h, ag_own), (mg_h, mg_own))]
    q_loads = [load(a, b) for a, b in ((q1_h, q1_w), (q2_h, q2_w), (tab_h, tab))]
    kv_loads = [load(a, b) for a, b in ((k1_h, k1_w), (k2_h, k2_w), (vw_h, vw_w))]
    k_loads = [load(kc_h.at[b], kc.at[b]) for b in range(ROWS)]
    v_loads = [load(vc_h.at[b], vc.at[b]) for b in range(ROWS)]
    late_loads = [
        load(a, b)
        for a, b in ((hsw_h, hsw), (hg_h, hg), (ow_h, ow_w), (gw_h, gw_w), (uw_h, uw_w), (dw_h, dw_w))
    ]
    for copy in first:
        copy.wait()
    pl.semaphore_wait(barrier, KV)

    sends = []

    def pair(k, src, dst):
        copy = pltpu.make_async_remote_copy(
            src, dst, pair_send.at[k], pair_recv.at[k], device_id=partner, device_id_type=MESH
        )
        copy.start()
        sends.append(copy)
        return copy

    def spread(source, landing, send_sem, recv_sem):
        for d, p in enumerate(peers):
            copy = pltpu.make_async_remote_copy(
                source(p), landing.at[kv], send_sem.at[d], recv_sem.at[kv],
                device_id=(dp, p, tp), device_id_type=MESH,
            )
            copy.start()
            sends.append(copy)

    def gathered(landing, recv_sem, send_sem):
        for d, p in enumerate(peers):
            pltpu.make_async_remote_copy(
                landing.at[p], landing.at[p], send_sem.at[d], recv_sem.at[p],
                device_id=(dp, p, tp), device_id_type=MESH,
            ).wait_recv()

    swaps = [pair(0, tok_own, tok_far), pair(1, ag_own, ag_far), pair(2, mg_own, mg_far)]
    lane = lax.broadcasted_iota(jnp.int32, (8, 128), 1)
    sub = lax.broadcasted_iota(jnp.int32, (8, 128), 0)
    diagonal = lane == sub
    for copy in q_loads:
        copy.wait()
    for copy in swaps:
        copy.wait_recv()

    def joined(own, far):
        own, far = own[...].astype(F32), far[...].astype(F32)
        return jnp.concatenate([jnp.where(tp == 0, own, far), jnp.where(tp == 0, far, own)], axis=-1)

    tokens = joined(tok_own, tok_far)
    scaled = (tokens * joined(ag_own, ag_far)).astype(BF16)
    mixer_gain = joined(mg_own, mg_far)
    square = jnp.sum(tokens * tokens, axis=1, keepdims=True)
    square_row = jnp.sum(jnp.where(diagonal, square, 0.0), axis=0, keepdims=True)
    for w, ref in enumerate((q1_w, q2_w)):
        part = jnp.dot(scaled, ref[...], preferred_element_type=F32)
        for t in range(2):
            qx[kv, 16 * w + 8 * t : 16 * w + 8 * t + 8, :] = part[:, 128 * t : 128 * t + 128]
    qx[kv, 32:33, :] = square_row
    spread(lambda p: qx.at[kv], qx, q_send, q_recv)

    for copy in kv_loads:
        copy.wait()
    for w, ref in enumerate((k1_w, k2_w)):
        part = jnp.dot(scaled, ref[...], preferred_element_type=F32)
        for t in range(2):
            ax[kv, 16 * w + 8 * t : 16 * w + 8 * t + 8, :] = part[:, 128 * t : 128 * t + 128]
    part = jnp.dot(scaled, vw_w[...], preferred_element_type=F32)
    for t in range(HEADS):
        ax[kv, 32 + 8 * t : 40 + 8 * t, :] = part[:, 128 * t : 128 * t + 128]
    spread(lambda p: ax.at[kv], ax, a_send, a_recv)

    gathered(qx, q_recv, q_send)

    def ratio_of(total):
        return lax.rsqrt(total / D + NORM_EPSILON)

    square_total = qx[0, 32:33, :]
    for s in range(1, KV):
        square_total = square_total + qx[s, 32:33, :]
    ratio_row = ratio_of(square_total)
    ratio = jnp.sum(jnp.where(diagonal, ratio_row, 0.0), axis=1, keepdims=True)
    cosine, sine = tab[0:1, :], tab[1:2, :]
    lead = lax.rem(lane, DH) < DH // 2

    def rotated(x):
        turned = jnp.where(lead, pltpu.roll(x, 128 - DH // 2, 1), pltpu.roll(x, DH // 2, 1))
        return (x * cosine + turned * sine).astype(BF16).astype(F32)

    def total_of(ref, at):
        total = ref[0, at : at + 8, :]
        for s in range(1, KV):
            total = total + ref[s, at : at + 8, :]
        return total

    query = [[rotated(total_of(qx, 16 * m + 8 * t) * ratio) for t in range(2)] for m in range(2)]
    low = lane < DH
    for h in range(HEADS):
        for m in range(2):
            x = query[m][h // 2]
            if h % 2 != m:
                x = pltpu.roll(x, DH, 1)
            qs[pl.ds(2 * h + m, 8, stride=8), :] = jnp.where(low if m == 0 else ~low, x, 0.0)

    key_head = lax.rem(lax.broadcasted_iota(jnp.int32, (16, 128), 1), HEADS)
    row_head = lax.rem(lax.broadcasted_iota(jnp.int32, (16, 128), 0), 8) // 2
    own_head = key_head == row_head
    scale = DH ** (-0.5)
    zero = jnp.zeros((8, 128), F32)
    peaks, sums = zero, zero
    for b in range(0, ROWS, 2):
        for copy in k_loads[b : b + 2]:
            copy.wait()
        left = jnp.concatenate(
            [
                jnp.concatenate([qs[8 * b : 8 * b + 8, :], zero], axis=1),
                jnp.concatenate([zero, qs[8 * b + 8 : 8 * b + 16, :]], axis=1),
            ],
            axis=0,
        ).astype(BF16)
        scores = []
        peak = jnp.full((16, 128), FLOOR, F32)
        step = 1024
        for c in range(0, KEYS, step):
            keys = jnp.concatenate([kc[b, c : c + step, :], kc[b + 1, c : c + step, :]], axis=1)
            s = lax.dot_general(left, keys, (((1,), (1,)), ((), ())), preferred_element_type=F32)
            for t in range(0, step, 128):
                one = jnp.where(own_head, s[:, t : t + 128], FLOOR)
                peak = jnp.maximum(peak, one)
                scores.append(one)
        peak = jnp.max(peak, axis=1, keepdims=True)
        total = jnp.zeros((16, 128), F32)
        weights = []
        for one in scores:
            e = jnp.exp((one - peak) * scale)
            total = total + e
            weights.append(e.astype(BF16))
        total = jnp.sum(total, axis=1, keepdims=True)
        for copy in v_loads[b : b + 2]:
            copy.wait()
        acc = jnp.zeros((16, 256), F32)
        for c in range(0, KEYS, step):
            values = jnp.concatenate([vc[b, c : c + step, :], vc[b + 1, c : c + step, :]], axis=1)
            w = jnp.concatenate(weights[c // 128 : (c + step) // 128], axis=1)
            acc = acc + jnp.dot(w, values, preferred_element_type=F32)
        for k in range(2):
            at = 8 * k
            cx[kv, pl.ds(b + k, 8, stride=8), :] = acc[at : at + 8, 128 * k : 128 * k + 128]
            for value, base in ((peak * scale, 0), (total, 8)):
                column = value[at : at + 8]
                row = jnp.sum(jnp.where(lane - base == sub, column, 0.0), axis=0, keepdims=True)
                if base == 0:
                    peaks = jnp.where(sub == b + k, row, peaks)
                else:
                    sums = jnp.where(sub == b + k, row, sums)
    cx[kv, 64:72, :] = jnp.where(lane < 8, peaks, sums)
    spread(lambda p: cx.at[kv], cx, c_send, c_recv)

    gathered(ax, a_recv, a_send)
    own_scores, new_values = [], []
    for m in range(2):
        for t in range(2):
            product = query[m][t] * rotated(total_of(ax, 16 * m + 8 * t) * ratio)
            for k in range(2):
                half = jnp.sum(jnp.where(low if k == 0 else ~low, product, 0.0), axis=1, keepdims=True)
                own_scores.append((2 * t + k, m, half * scale))
    own_scores = {(h, m): s for h, m, s in own_scores}
    for h in range(HEADS):
        new_values.append((total_of(ax, 32 + 8 * h) * ratio).astype(BF16).astype(F32))
    own = zero
    for h in range(HEADS):
        for m in range(2):
            own = jnp.where(lane == 2 * h + m, own_scores[h, m], own)
    for copy in late_loads[:3]:
        copy.wait()

    gathered(cx, c_recv, c_send)
    stats = [cx[s, 64:72, :] for s in range(KV)]
    peak = own
    for s in stats:
        peak = jnp.maximum(peak, s)
    own_weight = jnp.exp(own - peak)
    factors = [jnp.exp(s - peak) for s in stats]
    weight_sum = own_weight
    for f, s in zip(factors, stats):
        weight_sum = weight_sum + f * pltpu.roll(s, 120, 1)
    inverse = 1.0 / weight_sum
    attended = []
    for h in range(HEADS):
        averaged = []
        for m in range(2):
            c = 2 * h + m
            acc = own_weight[:, c : c + 1] * new_values[h]
            for s in range(KV):
                acc = acc + factors[s][:, c : c + 1] * cx[s, 8 * c : 8 * c + 8, :]
            averaged.append(acc * inverse[:, c : c + 1])
        difference = averaged[0] - hsw[0:1, h : h + 1] * averaged[1]
        norm = lax.rsqrt(jnp.mean(difference * difference, axis=1, keepdims=True) + HEAD_EPSILON)
        attended.append((difference * norm * hg[...] * HEAD_SCALE).astype(BF16))
    attended = jnp.concatenate(attended, axis=1)
    os_own[...] = jnp.dot(attended, ow_w[...], preferred_element_type=F32).astype(BF16)
    swap = pair(3, os_own, os_far)
    for copy in late_loads[3:]:
        copy.wait()
    swap.wait_recv()
    mixed = (tokens + (os_own[...].astype(F32) + os_far[...].astype(F32))).astype(BF16).astype(F32)
    mixer_scaled = (mixed * mixer_gain).astype(BF16)
    square = jnp.broadcast_to(jnp.sum(mixed * mixed, axis=1, keepdims=True), (8, 128))
    for w, ref in enumerate((gw_w, uw_w)):
        part = jnp.dot(mixer_scaled, ref[...], preferred_element_type=F32)
        for t in range(FT):
            row = (t // HT) * GR + w * HT + t % HT
            gs[pl.ds(row, 8, stride=2 * GR), :] = part[:, 128 * t : 128 * t + 128]
    for half in range(2):
        gs[pl.ds(half * GR + 2 * HT, 8, stride=2 * GR), :] = square
    gx[kv] = gs[pl.ds(pl.multiple_of(kv * GR, 8), GR), :]
    spread(lambda p: gs.at[pl.ds(pl.multiple_of(p * GR, 8), GR), :], gx, g_send, g_recv)
    gathered(gx, g_recv, g_send)
    total = gx[0]
    for s in range(1, KV):
        total = total + gx[s]
    mixer_ratio = ratio_of(total[2 * HT : 2 * HT + 1])
    gate = total[:HT] * mixer_ratio
    up = total[HT : 2 * HT] * mixer_ratio
    hidden = gate / (1.0 + jnp.exp(-gate)) * up
    hx[kv, 0:HT, :] = hidden.astype(BF16)
    spread(lambda p: hx.at[kv], hx, h_send, h_recv)
    gathered(hx, h_recv, h_send)
    for s in range(KV):
        hs[16 * s : 16 * s + 16, :] = hx[s].astype(F32)
    hidden = jnp.concatenate(
        [hs[pl.ds(16 * (t // HT) + t % HT, 8, stride=32), :].astype(BF16) for t in range(FT)], axis=1
    )
    ds_own[...] = jnp.dot(hidden, dw_w[...], preferred_element_type=F32).astype(BF16)
    swap = pair(4, ds_own, ds_far)
    swap.wait_recv()
    result = mixed + (ds_own[...].astype(F32) + ds_far[...].astype(F32))
    result = jnp.where(tp == 0, result, pltpu.roll(result, DH, 1))
    out_ref[...] = result[:, :64].astype(BF16)
    for copy in sends:
        copy.wait_send()


def shards(
    tokens, attention_gain, query_one, query_two, key_one, key_two, value_weight, head_second_weight, head_gain,
    out_weight, mixer_gain, gate_weight, up_weight, down_weight, key_cache, value_cache,
):
    any_space = pl.BlockSpec(memory_space=pl.ANY)
    vmem = pltpu.VMEM
    dma = pltpu.SemaphoreType.DMA
    return pl.pallas_call(
        layer_kernel,
        out_shape=jax.ShapeDtypeStruct((ROWS, 64), BF16),
        in_specs=[any_space] * 17,
        out_specs=pl.BlockSpec(memory_space=pltpu.VMEM),
        scratch_shapes=[
            vmem((ROWS, 64), BF16), vmem((ROWS, 64), BF16),
            vmem((1, 64), BF16), vmem((1, 64), BF16), vmem((1, 64), BF16), vmem((1, 64), BF16),
            vmem((128, 256), BF16), vmem((128, 256), BF16), vmem((128, 256), BF16), vmem((128, 256), BF16),
            vmem((128, 512), BF16), vmem((1, HEADS), F32), vmem((1, 128), F32), vmem((512, 128), BF16),
            vmem((128, FF), BF16), vmem((128, FF), BF16), vmem((FF, 128), BF16),
            vmem((ROWS, KEYS, 128), BF16), vmem((ROWS, KEYS, 128), BF16), vmem((8, 128), F32),
            vmem((KV, QR, 128), F32), vmem((KV, 64, 128), F32), vmem((KV, CR, 128), F32),
            vmem((KV * GR, 128), F32), vmem((KV, GR, 128), F32),
            vmem((KV, 16, 128), BF16), vmem((KV * 16, 128), F32), vmem((64, 128), F32),
            vmem((8, 128), BF16), vmem((8, 128), BF16), vmem((8, 128), BF16), vmem((8, 128), BF16),
            dma((31,)), dma((5,)), dma((5,)),
            dma((KV,)), dma((KV,)), dma((KV,)), dma((KV,)), dma((KV,)), dma((KV,)),
            dma((KV,)), dma((KV,)), dma((KV,)), dma((KV,)),
        ],
        compiler_params=pltpu.CompilerParams(
            collective_id=0, has_side_effects=True, vmem_limit_bytes=60 * 1024 * 1024
        ),
        name="layer",
    )(
        tokens, attention_gain.reshape(1, -1), query_one, query_two, key_one, key_two, value_weight,
        head_second_weight.reshape(1, -1), head_gain.reshape(1, -1), out_weight, mixer_gain.reshape(1, -1),
        gate_weight, up_weight, down_weight,
        key_cache.reshape(ROWS, KEYS, 128), value_cache.reshape(ROWS, KEYS, 128), jnp.asarray(rotary_tables()),
    )


def solution(mesh):
    both = ("kv", "tp")
    return jax.shard_map(
        shards,
        mesh=mesh,
        in_specs=(
            P("dp", both), P(both), P("kv", "tp"), P("kv", "tp"), P("kv", "tp"), P("kv", "tp"), P("kv", "tp"),
            P("tp"), P(), P("tp", "kv"), P(both), P("kv", "tp"), P("kv", "tp"), P("tp", "kv"),
            P("dp", "kv", "tp", None), P("dp", "kv", "tp", None),
        ),
        out_specs=P("dp", both),
        check_vma=False,
    )
```

time: 120 us -> 49.7 us (0.41)
  blocking collectives: 50.7 us -> 0 us
  Pallas kernels: 0 us -> 48.3 us
  waiting for transfers between devices: 25.7 us -> 0 us
  matrix products: 16.4 us -> 0 us
  starting transfers between devices: 14.9 us -> 0 us
  local copies, waits for them, and re-layouts: 7.53 us -> 1.26 us
  other arithmetic: 3.79 us -> 0 us
    pallas_call x0 -> x1, Pallas kernels: none -> 48.3 us  [shards(): pl.pallas_call(layer_kernel, out_shape=jax.ShapeDtypeStruct((ROWS, 64), B...]
    all_to_all x3 -> x0, blocking collectives: 26.8 us -> none  [the longest x2 17.4 us: sent_and_summed(): lax.all_to_all(parts, axis, split_axis=0, concat_axis=0, tiled=True)]
    all_to_all x3 -> x0, waiting for transfers between devices: 25.7 us -> none  [the longest x1 12.8 us: copy_for_each(): return lax.all_to_all(copies, axis, split_axis=0, concat_axis=0, tiled=True)]
    all_gather x4 -> x0, blocking collectives: 23.8 us -> none  [the longest x2 19.2 us: collected_together(): both, at, found = (lax.all_gather(jnp.concatenate(lines), axis), 0, {})]
    dot_general x11 -> x0, matrix products: 16.4 us -> none  [the longest x1 5.74 us: shards(): jnp.einsum('bhmk,bphk->bhmp', padded_query_rows, key_cache, preferred_ele...]
    all_to_all x3 -> x0, starting transfers between devices: 14.9 us -> none  [the longest x1 7.88 us: copy_for_each(): return lax.all_to_all(copies, axis, split_axis=0, concat_axis=0, tiled=True)]
    squeeze x16 -> x0, local copies, waits for them, and re-layouts: 2.01 us -> none  [the longest x12 1.51 us: joined_all(): value = combine(value, jax.tree.map(lambda part: part[k], pieces))]
    reshape x17 -> x0, local copies, waits for them, and re-layouts: 1.94 us -> none  [the longest x6 1.23 us: split_up(): return jnp.moveaxis(value.reshape(*before, devices, -1, *after), dim, 0)]
  transfers between devices with their start and end apart: 3 -> 0, of which waited for: 3 -> 0; matrix products, arithmetic and copies ran while one was open for 2% -> 0% of each run, Pallas kernels for 0% -> 0%
where the time goes in v1:
time: 49.7 us; the launch traced here: 49.6 us
  Pallas kernels  48.3 us (97%)
  local copies, waits for them, and re-layouts  1.26 us (3%)
    pallas_call x1, Pallas kernels, shards(): pl.pallas_call(layer_kernel, out_shape=jax.ShapeDtypeStruct((ROWS, 64), B...  48.3 us
    unnamed x1, local copies, waits for them, and re-layouts  1.26 us

profile of v1, /device:TPU:1, one launch (start us, length us, event | category | flops | bytes accessed | tf_op | source)
XLA Modules:
  0.0 49.6 jit_solution(13680934302403695883)
XLA Ops:
  0.0 48.3 %layer.1 = bf16[8,64]{1,0:T(8,128)(2,1)} custom-call(bf16[8,64]{1,0:T(8,128)(2,1)} %tok_h.1, bf16[1,64]{1,0:T(2,128)(2,1)} %bitcast.8, bf16[128,256]{1,0:T(8,128)(2,1)} %q1_h.1, bf16[128,256]{1,0:T(8,128)(2,1)} %q2_h.1, bf16[128,256]{1,0:T(8,128)(2,1)} %k1_h.1, bf16[128,256]{1,0:T(8,128)(2,1)} %k2_h.1, bf16[128,512]{1,0:T(8,128)(2,1)} %vw_h.1, ...), custom_call_target="tpu_custom_call" | custom-call | tf_op jit(solution)/shard_map/layer/pallas_call | solution.py:323
  48.3 1.3 %copy.19 = bf16[8,64]{1,0:T(8,128)(2,1)} copy(bf16[8,64]{1,0:T(8,128)(2,1)} %layer.1) | data formatting | bytes 2048

commit v2 on v1

--- a/solution.py
+++ b/solution.py
@@ -26,7 +26,6 @@
 FLOOR = -1e30
 KEYS = POSITIONS * HEADS
 QR = 33
-CR = 72
 GR = 24
 
 
@@ -48,8 +47,8 @@
     out_ref,
     tok_own, tok_far, ag_own, ag_far, mg_own, mg_far,
     q1_w, q2_w, k1_w, k2_w, vw_w, hsw, hg, ow_w, gw_w, uw_w, dw_w, kc, vc, tab,
-    qx, ax, cx, gs, gx, hx, hs, qs, os_own, os_far, ds_own, ds_far,
-    load_sem, pair_send, pair_recv, q_send, q_recv, a_send, a_recv, c_send, c_recv, g_send, g_recv, h_send, h_recv,
+    qx, rs, rx, nx, cx, sx, gs, gx, hx, hs, qs, nv, sc, df, os_own, os_far, ds_own, ds_far,
+    load_sem, pair_send, pair_recv, all_send, all_recv,
 ):
     dp, kv, tp = (lax.axis_index(a) for a in ("dp", "kv", "tp"))
     barrier = pltpu.get_barrier_semaphore()
@@ -70,8 +69,7 @@
     first = [load(a, b) for a, b in ((tok_h, tok_own), (ag_h, ag_own), (mg_h, mg_own))]
     q_loads = [load(a, b) for a, b in ((q1_h, q1_w), (q2_h, q2_w), (tab_h, tab))]
     kv_loads = [load(a, b) for a, b in ((k1_h, k1_w), (k2_h, k2_w), (vw_h, vw_w))]
-    k_loads = [load(kc_h.at[b], kc.at[b]) for b in range(ROWS)]
-    v_loads = [load(vc_h.at[b], vc.at[b]) for b in range(ROWS)]
+    cache_loads = [load(kc_h, kc), load(vc_h, vc)]
     late_loads = [
         load(a, b)
         for a, b in ((hsw_h, hsw), (hg_h, hg), (ow_h, ow_w), (gw_h, gw_w), (uw_h, uw_w), (dw_h, dw_w))
@@ -80,7 +78,7 @@
         copy.wait()
     pl.semaphore_wait(barrier, KV)
 
-    sends = []
+    sends, spreads = [], []
 
     def pair(k, src, dst):
         copy = pltpu.make_async_remote_copy(
@@ -90,21 +88,20 @@
         sends.append(copy)
         return copy
 
-    def spread(source, landing, send_sem, recv_sem):
-        for d, p in enumerate(peers):
-            copy = pltpu.make_async_remote_copy(
-                source(p), landing.at[kv], send_sem.at[d], recv_sem.at[kv],
+    def spread(stage, source, target):
+        for p in peers:
+            pltpu.make_async_remote_copy(
+                source(p), target, all_send.at[stage], all_recv.at[stage],
                 device_id=(dp, p, tp), device_id_type=MESH,
-            )
-            copy.start()
-            sends.append(copy)
-
-    def gathered(landing, recv_sem, send_sem):
-        for d, p in enumerate(peers):
-            pltpu.make_async_remote_copy(
-                landing.at[p], landing.at[p], send_sem.at[d], recv_sem.at[p],
-                device_id=(dp, p, tp), device_id_type=MESH,
-            ).wait_recv()
+            ).start()
+
+    def everything(stage, landing):
+        most = landing.at[0 : KV - 1]
+        copy = pltpu.make_async_remote_copy(
+            most, most, all_send.at[stage], all_recv.at[stage], device_id=partner, device_id_type=MESH
+        )
+        spreads.append(copy)
+        copy.wait_recv()
 
     swaps = [pair(0, tok_own, tok_far), pair(1, ag_own, ag_far), pair(2, mg_own, mg_far)]
     lane = lax.broadcasted_iota(jnp.int32, (8, 128), 1)
@@ -129,20 +126,23 @@
         for t in range(2):
             qx[kv, 16 * w + 8 * t : 16 * w + 8 * t + 8, :] = part[:, 128 * t : 128 * t + 128]
     qx[kv, 32:33, :] = square_row
-    spread(lambda p: qx.at[kv], qx, q_send, q_recv)
+    spread(0, lambda p: qx.at[kv], qx.at[kv])
 
     for copy in kv_loads:
         copy.wait()
     for w, ref in enumerate((k1_w, k2_w)):
         part = jnp.dot(scaled, ref[...], preferred_element_type=F32)
         for t in range(2):
-            ax[kv, 16 * w + 8 * t : 16 * w + 8 * t + 8, :] = part[:, 128 * t : 128 * t + 128]
+            rs[pl.ds(8 * t + w, 8, stride=16), :] = part[:, 128 * t : 128 * t + 128]
     part = jnp.dot(scaled, vw_w[...], preferred_element_type=F32)
     for t in range(HEADS):
-        ax[kv, 32 + 8 * t : 40 + 8 * t, :] = part[:, 128 * t : 128 * t + 128]
-    spread(lambda p: ax.at[kv], ax, a_send, a_recv)
-
-    gathered(qx, q_recv, q_send)
+        rs[pl.ds(8 * (t // 2) + 2 + t % 2, 8, stride=16), :] = part[:, 128 * t : 128 * t + 128]
+    rx[kv] = rs[pl.ds(pl.multiple_of(8 * kv, 8), 8), :]
+    spread(1, lambda p: rs.at[pl.ds(pl.multiple_of(8 * p, 8), 8), :], rx.at[kv])
+
+    for copy in cache_loads:
+        copy.wait()
+    everything(0, qx)
 
     def ratio_of(total):
         return lax.rsqrt(total / D + NORM_EPSILON)
@@ -179,10 +179,10 @@
     own_head = key_head == row_head
     scale = DH ** (-0.5)
     zero = jnp.zeros((8, 128), F32)
-    peaks, sums = zero, zero
-    for b in range(0, ROWS, 2):
-        for copy in k_loads[b : b + 2]:
-            copy.wait()
+    step = 1024
+
+    def score(pair_index):
+        b = 2 * pair_index
         left = jnp.concatenate(
             [
                 jnp.concatenate([qs[8 * b : 8 * b + 8, :], zero], axis=1),
@@ -190,64 +190,76 @@
             ],
             axis=0,
         ).astype(BF16)
-        scores = []
         peak = jnp.full((16, 128), FLOOR, F32)
-        step = 1024
         for c in range(0, KEYS, step):
             keys = jnp.concatenate([kc[b, c : c + step, :], kc[b + 1, c : c + step, :]], axis=1)
             s = lax.dot_general(left, keys, (((1,), (1,)), ((), ())), preferred_element_type=F32)
             for t in range(0, step, 128):
                 one = jnp.where(own_head, s[:, t : t + 128], FLOOR)
                 peak = jnp.maximum(peak, one)
-                scores.append(one)
-        peak = jnp.max(peak, axis=1, keepdims=True)
+                sc[pair_index % 2, :, c + t : c + t + 128] = one
+        return peak
+
+    stat = zero
+    running = score(0)
+    for pair_index in range(ROWS // 2):
+        b = 2 * pair_index
+        peak = jnp.max(running, axis=1, keepdims=True)
+        if pair_index + 1 < ROWS // 2:
+            running = score(pair_index + 1)
         total = jnp.zeros((16, 128), F32)
         weights = []
-        for one in scores:
-            e = jnp.exp((one - peak) * scale)
+        for t in range(0, KEYS, 128):
+            e = jnp.exp((sc[pair_index % 2, :, t : t + 128] - peak) * scale)
             total = total + e
             weights.append(e.astype(BF16))
         total = jnp.sum(total, axis=1, keepdims=True)
-        for copy in v_loads[b : b + 2]:
-            copy.wait()
+        for k in range(2):
+            stat = jnp.where(lane == b + k, peak[8 * k : 8 * k + 8] * scale, stat)
+            stat = jnp.where(lane == 8 + b + k, total[8 * k : 8 * k + 8], stat)
+        if pair_index + 1 == ROWS // 2:
+            sx[kv] = stat
+            spread(2, lambda p: sx.at[kv], sx.at[kv])
         acc = jnp.zeros((16, 256), F32)
         for c in range(0, KEYS, step):
             values = jnp.concatenate([vc[b, c : c + step, :], vc[b + 1, c : c + step, :]], axis=1)
             w = jnp.concatenate(weights[c // 128 : (c + step) // 128], axis=1)
             acc = acc + jnp.dot(w, values, preferred_element_type=F32)
-        for k in range(2):
-            at = 8 * k
-            cx[kv, pl.ds(b + k, 8, stride=8), :] = acc[at : at + 8, 128 * k : 128 * k + 128]
-            for value, base in ((peak * scale, 0), (total, 8)):
-                column = value[at : at + 8]
-                row = jnp.sum(jnp.where(lane - base == sub, column, 0.0), axis=0, keepdims=True)
-                if base == 0:
-                    peaks = jnp.where(sub == b + k, row, peaks)
-                else:
-                    sums = jnp.where(sub == b + k, row, sums)
-    cx[kv, 64:72, :] = jnp.where(lane < 8, peaks, sums)
-    spread(lambda p: cx.at[kv], cx, c_send, c_recv)
-
-    gathered(ax, a_recv, a_send)
-    own_scores, new_values = [], []
+        place = pl.ds(8 * b, 16)
+        cx[kv, place, :] = jnp.concatenate([acc[0:8, 0:128], acc[8:16, 128:256]], axis=0).astype(BF16)
+        spread(3, lambda p: cx.at[kv, place], cx.at[kv, place])
+        if pair_index == 1:
+            everything(1, rx)
+            nx[pl.ds(pl.multiple_of(8 * kv, 8), 8), :] = total_of(rx, 0)
+            mine = nx.at[pl.ds(pl.multiple_of(8 * kv, 8), 8), :]
+            spread(4, lambda p: mine, mine)
+
+    most = nx.at[0 : 8 * (KV - 1)]
+    copy = pltpu.make_async_remote_copy(
+        most, most, all_send.at[4], all_recv.at[4], device_id=partner, device_id_type=MESH
+    )
+    spreads.append(copy)
+    copy.wait_recv()
+    own = zero
     for m in range(2):
         for t in range(2):
-            product = query[m][t] * rotated(total_of(ax, 16 * m + 8 * t) * ratio)
+            product = query[m][t] * rotated(nx[pl.ds(8 * t + m, 8, stride=16), :] * ratio)
             for k in range(2):
                 half = jnp.sum(jnp.where(low if k == 0 else ~low, product, 0.0), axis=1, keepdims=True)
-                own_scores.append((2 * t + k, m, half * scale))
-    own_scores = {(h, m): s for h, m, s in own_scores}
+                row = jnp.sum(jnp.where(diagonal, half, 0.0), axis=0, keepdims=True)
+                own = jnp.where(sub == 2 * (2 * t + k) + m, row * scale, own)
     for h in range(HEADS):
-        new_values.append((total_of(ax, 32 + 8 * h) * ratio).astype(BF16).astype(F32))
-    own = zero
+        value = (nx[pl.ds(8 * (h // 2) + 2 + h % 2, 8, stride=16), :] * ratio).astype(BF16).astype(F32)
+        for m in range(2):
+            nv[pl.ds(2 * h + m, 8, stride=8), :] = value
+    for copy in late_loads[:3]:
+        copy.wait()
+    second = jnp.zeros((8, 1), F32)
     for h in range(HEADS):
-        for m in range(2):
-            own = jnp.where(lane == 2 * h + m, own_scores[h, m], own)
-    for copy in late_loads[:3]:
-        copy.wait()
-
-    gathered(cx, c_recv, c_send)
-    stats = [cx[s, 64:72, :] for s in range(KV)]
+        second = jnp.where(sub[:, :1] == 2 * h, hsw[0:1, h : h + 1], second)
+
+    everything(2, sx)
+    stats = [sx[s] for s in range(KV)]
     peak = own
     for s in stats:
         peak = jnp.maximum(peak, s)
@@ -257,19 +269,19 @@
     for f, s in zip(factors, stats):
         weight_sum = weight_sum + f * pltpu.roll(s, 120, 1)
     inverse = 1.0 / weight_sum
-    attended = []
-    for h in range(HEADS):
-        averaged = []
-        for m in range(2):
-            c = 2 * h + m
-            acc = own_weight[:, c : c + 1] * new_values[h]
-            for s in range(KV):
-                acc = acc + factors[s][:, c : c + 1] * cx[s, 8 * c : 8 * c + 8, :]
-            averaged.append(acc * inverse[:, c : c + 1])
-        difference = averaged[0] - hsw[0:1, h : h + 1] * averaged[1]
-        norm = lax.rsqrt(jnp.mean(difference * difference, axis=1, keepdims=True) + HEAD_EPSILON)
-        attended.append((difference * norm * hg[...] * HEAD_SCALE).astype(BF16))
-    attended = jnp.concatenate(attended, axis=1)
+    everything(3, cx)
+    for b in range(0, ROWS, 2):
+        acc = [own_weight[:, b + k : b + k + 1] * nv[8 * (b + k) : 8 * (b + k) + 8, :] for k in range(2)]
+        for s in range(KV):
+            part = cx[s, 8 * b : 8 * b + 16, :].astype(F32)
+            for k in range(2):
+                acc[k] = acc[k] + factors[s][:, b + k : b + k + 1] * part[8 * k : 8 * k + 8]
+        for k in range(2):
+            averaged = acc[k] * inverse[:, b + k : b + k + 1]
+            difference = averaged - second * pltpu.roll(averaged, 7, 0)
+            norm = lax.rsqrt(jnp.mean(difference * difference, axis=1, keepdims=True) + HEAD_EPSILON)
+            df[8 * (b + k) : 8 * (b + k) + 8, :] = difference * norm * hg[...] * HEAD_SCALE
+    attended = jnp.concatenate([df[pl.ds(2 * h, 8, stride=8), :].astype(BF16) for h in range(HEADS)], axis=1)
     os_own[...] = jnp.dot(attended, ow_w[...], preferred_element_type=F32).astype(BF16)
     swap = pair(3, os_own, os_far)
     for copy in late_loads[3:]:
@@ -286,8 +298,8 @@
     for half in range(2):
         gs[pl.ds(half * GR + 2 * HT, 8, stride=2 * GR), :] = square
     gx[kv] = gs[pl.ds(pl.multiple_of(kv * GR, 8), GR), :]
-    spread(lambda p: gs.at[pl.ds(pl.multiple_of(p * GR, 8), GR), :], gx, g_send, g_recv)
-    gathered(gx, g_recv, g_send)
+    spread(5, lambda p: gs.at[pl.ds(pl.multiple_of(p * GR, 8), GR), :], gx.at[kv])
+    everything(5, gx)
     total = gx[0]
     for s in range(1, KV):
         total = total + gx[s]
@@ -296,8 +308,8 @@
     up = total[HT : 2 * HT] * mixer_ratio
     hidden = gate / (1.0 + jnp.exp(-gate)) * up
     hx[kv, 0:HT, :] = hidden.astype(BF16)
-    spread(lambda p: hx.at[kv], hx, h_send, h_recv)
-    gathered(hx, h_recv, h_send)
+    spread(6, lambda p: hx.at[kv], hx.at[kv])
+    everything(6, hx)
     for s in range(KV):
         hs[16 * s : 16 * s + 16, :] = hx[s].astype(F32)
     hidden = jnp.concatenate(
@@ -309,7 +321,7 @@
     result = mixed + (ds_own[...].astype(F32) + ds_far[...].astype(F32))
     result = jnp.where(tp == 0, result, pltpu.roll(result, DH, 1))
     out_ref[...] = result[:, :64].astype(BF16)
-    for copy in sends:
+    for copy in sends + spreads:
         copy.wait_send()
 
 
@@ -332,13 +344,13 @@
             vmem((128, 512), BF16), vmem((1, HEADS), F32), vmem((1, 128), F32), vmem((512, 128), BF16),
             vmem((128, FF), BF16), vmem((128, FF), BF16), vmem((FF, 128), BF16),
             vmem((ROWS, KEYS, 128), BF16), vmem((ROWS, KEYS, 128), BF16), vmem((8, 128), F32),
-            vmem((KV, QR, 128), F32), vmem((KV, 64, 128), F32), vmem((KV, CR, 128), F32),
+            vmem((KV, QR, 128), F32), vmem((KV * 8, 128), F32), vmem((KV, 8, 128), F32), vmem((KV * 8, 128), F32),
+            vmem((KV, 64, 128), BF16), vmem((KV, 8, 128), F32),
             vmem((KV * GR, 128), F32), vmem((KV, GR, 128), F32),
-            vmem((KV, 16, 128), BF16), vmem((KV * 16, 128), F32), vmem((64, 128), F32),
+            vmem((KV, 16, 128), BF16), vmem((KV * 16, 128), F32), vmem((64, 128), F32), vmem((64, 128), F32),
+            vmem((2, 16, KEYS), F32), vmem((64, 128), F32),
             vmem((8, 128), BF16), vmem((8, 128), BF16), vmem((8, 128), BF16), vmem((8, 128), BF16),
-            dma((31,)), dma((5,)), dma((5,)),
-            dma((KV,)), dma((KV,)), dma((KV,)), dma((KV,)), dma((KV,)), dma((KV,)),
-            dma((KV,)), dma((KV,)), dma((KV,)), dma((KV,)),
+            dma((17,)), dma((5,)), dma((5,)), dma((7,)), dma((7,)),
         ],
         compiler_params=pltpu.CompilerParams(
             collective_id=0, has_side_effects=True, vmem_limit_bytes=60 * 1024 * 1024

time: 49.7 us -> 41.3 us (0.83)
  Pallas kernels: 48.3 us -> 39.9 us
    pallas_call x1, Pallas kernels: 48.3 us -> 39.9 us  [shards(): pl.pallas_call(layer_kernel, out_shape=jax.ShapeDtypeStruct((ROWS, 64), B...]
where the time goes in v2:
time: 41.3 us; the launch traced here: 41.1 us
  Pallas kernels  39.9 us (97%)
  local copies, waits for them, and re-layouts  1.26 us (3%)
    pallas_call x1, Pallas kernels, shards(): pl.pallas_call(layer_kernel, out_shape=jax.ShapeDtypeStruct((ROWS, 64), B...  39.9 us
    unnamed x1, local copies, waits for them, and re-layouts  1.26 us

profile of v2, /device:TPU:1, one launch (start us, length us, event | category | flops | bytes accessed | tf_op | source)
XLA Modules:
  0.0 41.1 jit_solution(8264459289972447421)
XLA Ops:
  0.0 39.9 %layer.1 = bf16[8,64]{1,0:T(8,128)(2,1)} custom-call(bf16[8,64]{1,0:T(8,128)(2,1)} %tok_h.1, bf16[1,64]{1,0:T(2,128)(2,1)} %bitcast.8, bf16[128,256]{1,0:T(8,128)(2,1)} %q1_h.1, bf16[128,256]{1,0:T(8,128)(2,1)} %q2_h.1, bf16[128,256]{1,0:T(8,128)(2,1)} %k1_h.1, bf16[128,256]{1,0:T(8,128)(2,1)} %k2_h.1, bf16[128,512]{1,0:T(8,128)(2,1)} %vw_h.1, ...), custom_call_target="tpu_custom_call" | custom-call | tf_op jit(solution)/shard_map/layer/pallas_call | solution.py:335
  39.9 1.3 %copy.19 = bf16[8,64]{1,0:T(8,128)(2,1)} copy(bf16[8,64]{1,0:T(8,128)(2,1)} %layer.1) | data formatting | bytes 2048

commit v3 on v2

--- a/solution.py
+++ b/solution.py
@@ -24,9 +24,16 @@
 HEAD_EPSILON = 1e-05
 HEAD_SCALE = 0.8
 FLOOR = -1e30
+LOG2E = 1.4426950408889634
 KEYS = POSITIONS * HEADS
 QR = 33
 GR = 24
+
+
+OFFSETS = sorted(
+    ((i, j) for i in range(4) for j in range(4) if (i, j) != (0, 0)),
+    key=lambda o: -min(o[0], 4 - o[0]) - min(o[1], 4 - o[1]),
+)
 
 
 def rotary_tables():
@@ -47,13 +54,14 @@
     out_ref,
     tok_own, tok_far, ag_own, ag_far, mg_own, mg_far,
     q1_w, q2_w, k1_w, k2_w, vw_w, hsw, hg, ow_w, gw_w, uw_w, dw_w, kc, vc, tab,
-    qx, rs, rx, nx, cx, sx, gs, gx, hx, hs, qs, nv, sc, df, os_own, os_far, ds_own, ds_far,
+    unit, kt, qx, rs, rx, cx, sx, gs, gb, gx, hx, hs, qs, sc, df, os_own, os_far, ds_own, ds_far, out_v,
     load_sem, pair_send, pair_recv, all_send, all_recv,
 ):
     dp, kv, tp = (lax.axis_index(a) for a in ("dp", "kv", "tp"))
     barrier = pltpu.get_barrier_semaphore()
     partner = (dp, kv, 1 - tp)
-    peers = [lax.rem(kv + d, KV) for d in range(1, KV)]
+    across, along = kv // 4, lax.rem(kv, 4)
+    peers = [lax.rem(across + i, 4) * 4 + lax.rem(along + j, 4) for i, j in OFFSETS]
     for p in peers:
         pl.semaphore_signal(barrier, 1, device_id=(dp, p, tp), device_id_type=MESH)
     pl.semaphore_signal(barrier, 1, device_id=partner, device_id_type=MESH)
@@ -95,8 +103,7 @@
                 device_id=(dp, p, tp), device_id_type=MESH,
             ).start()
 
-    def everything(stage, landing):
-        most = landing.at[0 : KV - 1]
+    def everything(stage, most):
         copy = pltpu.make_async_remote_copy(
             most, most, all_send.at[stage], all_recv.at[stage], device_id=partner, device_id_type=MESH
         )
@@ -138,11 +145,23 @@
     for t in range(HEADS):
         rs[pl.ds(8 * (t // 2) + 2 + t % 2, 8, stride=16), :] = part[:, 128 * t : 128 * t + 128]
     rx[kv] = rs[pl.ds(pl.multiple_of(8 * kv, 8), 8), :]
-    spread(1, lambda p: rs.at[pl.ds(pl.multiple_of(8 * p, 8), 8), :], rx.at[kv])
-
-    for copy in cache_loads:
-        copy.wait()
-    everything(0, qx)
+    spread(1, lambda p: rs.at[pl.ds(pl.multiple_of(8 * p, 8), 4), :], rx.at[kv, 0:4])
+
+    wide = (256, 256)
+    unit[...] = (lax.broadcasted_iota(jnp.int32, wide, 0) == lax.broadcasted_iota(jnp.int32, wide, 1)).astype(BF16)
+    cache_loads[0].wait()
+
+    def turn(c, carry):
+        at = pl.multiple_of(c * 512, 512)
+        for b in range(0, ROWS, 2):
+            keys = jnp.concatenate([kc[b, pl.ds(at, 512), :], kc[b + 1, pl.ds(at, 512), :]], axis=1)
+            turned = lax.dot_general(unit[...], keys, (((1,), (1,)), ((), ())), preferred_element_type=F32)
+            kt[b // 2, :, pl.ds(at, 512)] = turned.astype(BF16)
+        return carry
+
+    lax.fori_loop(0, KEYS // 512, turn, 0)
+    cache_loads[1].wait()
+    everything(0, qx.at[0 : KV - 1])
 
     def ratio_of(total):
         return lax.rsqrt(total / D + NORM_EPSILON)
@@ -181,106 +200,121 @@
     zero = jnp.zeros((8, 128), F32)
     step = 1024
 
-    def score(pair_index):
-        b = 2 * pair_index
+    order = [lax.rem(across + 1 + t, 4) for t in range(ROWS // 2)]
+    slot = 64 * (2 * lax.rem(kv, 8) + kv // 8)
+
+    def score(t):
+        rows = qs[pl.ds(pl.multiple_of(16 * order[t], 16), 16), :]
         left = jnp.concatenate(
             [
-                jnp.concatenate([qs[8 * b : 8 * b + 8, :], zero], axis=1),
-                jnp.concatenate([zero, qs[8 * b + 8 : 8 * b + 16, :]], axis=1),
+                jnp.concatenate([rows[0:8], zero], axis=1),
+                jnp.concatenate([zero, rows[8:16]], axis=1),
             ],
             axis=0,
         ).astype(BF16)
         peak = jnp.full((16, 128), FLOOR, F32)
         for c in range(0, KEYS, step):
-            keys = jnp.concatenate([kc[b, c : c + step, :], kc[b + 1, c : c + step, :]], axis=1)
-            s = lax.dot_general(left, keys, (((1,), (1,)), ((), ())), preferred_element_type=F32)
-            for t in range(0, step, 128):
-                one = jnp.where(own_head, s[:, t : t + 128], FLOOR)
+            s = jnp.dot(left, kt[order[t], :, c : c + step], preferred_element_type=F32)
+            for i in range(0, step, 128):
+                one = jnp.where(own_head, s[:, i : i + 128], FLOOR)
                 peak = jnp.maximum(peak, one)
-                sc[pair_index % 2, :, c + t : c + t + 128] = one
-        return peak
+                sc[t % 2, :, c + i : c + i + 128] = one
+        return jnp.max(peak, axis=1, keepdims=True)
+
+    def new_token():
+        everything(1, rx.at[0 : KV - 1, 0:4])
+        row, share = kv // 2, lax.rem(kv, 2)
+        new = total_of(rx, 0) * jnp.sum(jnp.where(sub[:, :1] == row, ratio, 0.0), axis=0, keepdims=True)
+        asked = [
+            jnp.sum(
+                jnp.where(sub == row, jnp.where(share == 0, query[m][0], query[m][1]), 0.0), axis=0, keepdims=True
+            )
+            for m in range(2)
+        ]
+        product = jnp.where(sub == 0, asked[0], asked[1]) * rotated(new)
+        wide_row = lax.broadcasted_iota(jnp.int32, (16, 128), 0)
+        score_column = jnp.full((16, 1), FLOOR, F32)
+        for k in range(2):
+            half = jnp.sum(jnp.where(low if k == 0 else ~low, product, 0.0), axis=1, keepdims=True)
+            for m in range(2):
+                here = wide_row[:, :1] == 4 * along + 2 * k + m
+                score_column = jnp.where(here, half[m : m + 1], score_column)
+        new = new.astype(BF16).astype(F32)
+        return score_column, jnp.where(lax.rem(wide_row, 4) < 2, new[2:3], new[3:4])
 
     stat = zero
     running = score(0)
-    for pair_index in range(ROWS // 2):
-        b = 2 * pair_index
-        peak = jnp.max(running, axis=1, keepdims=True)
-        if pair_index + 1 < ROWS // 2:
-            running = score(pair_index + 1)
+    for t in range(ROWS // 2):
+        b = 2 * order[t]
+        peak = running
+        if t + 1 < ROWS // 2:
+            running = score(t + 1)
+        else:
+            own_score, own_value = new_token()
+            peak = jnp.maximum(peak, own_score)
         total = jnp.zeros((16, 128), F32)
         weights = []
-        for t in range(0, KEYS, 128):
-            e = jnp.exp((sc[pair_index % 2, :, t : t + 128] - peak) * scale)
+        for i in range(0, KEYS, 128):
+            e = jnp.exp2((sc[t % 2, :, i : i + 128] - peak) * (scale * LOG2E))
             total = total + e
             weights.append(e.astype(BF16))
         total = jnp.sum(total, axis=1, keepdims=True)
+        if t + 1 == ROWS // 2:
+            own_weight = jnp.exp2((own_score - peak) * (scale * LOG2E))
+            total = total + own_weight
         for k in range(2):
-            stat = jnp.where(lane == b + k, peak[8 * k : 8 * k + 8] * scale, stat)
-            stat = jnp.where(lane == 8 + b + k, total[8 * k : 8 * k + 8], stat)
-        if pair_index + 1 == ROWS // 2:
-            sx[kv] = stat
-            spread(2, lambda p: sx.at[kv], sx.at[kv])
+            at = 8 * (b + k)
+            stat = jnp.where(lane - at == sub, peak[8 * k : 8 * k + 8] * scale, stat)
+            stat = jnp.where(lane - 64 - at == sub, total[8 * k : 8 * k + 8], stat)
+        if t + 1 == ROWS // 2:
+            sx[pl.ds(kv, 1), :] = jnp.sum(stat, axis=0, keepdims=True)
+            spread(2, lambda p: sx.at[pl.ds(kv, 1), :], sx.at[pl.ds(kv, 1), :])
         acc = jnp.zeros((16, 256), F32)
         for c in range(0, KEYS, step):
             values = jnp.concatenate([vc[b, c : c + step, :], vc[b + 1, c : c + step, :]], axis=1)
             w = jnp.concatenate(weights[c // 128 : (c + step) // 128], axis=1)
             acc = acc + jnp.dot(w, values, preferred_element_type=F32)
-        place = pl.ds(8 * b, 16)
-        cx[kv, place, :] = jnp.concatenate([acc[0:8, 0:128], acc[8:16, 128:256]], axis=0).astype(BF16)
-        spread(3, lambda p: cx.at[kv, place], cx.at[kv, place])
-        if pair_index == 1:
-            everything(1, rx)
-            nx[pl.ds(pl.multiple_of(8 * kv, 8), 8), :] = total_of(rx, 0)
-            mine = nx.at[pl.ds(pl.multiple_of(8 * kv, 8), 8), :]
-            spread(4, lambda p: mine, mine)
-
-    most = nx.at[0 : 8 * (KV - 1)]
-    copy = pltpu.make_async_remote_copy(
-        most, most, all_send.at[4], all_recv.at[4], device_id=partner, device_id_type=MESH
-    )
-    spreads.append(copy)
-    copy.wait_recv()
-    own = zero
-    for m in range(2):
-        for t in range(2):
-            product = query[m][t] * rotated(nx[pl.ds(8 * t + m, 8, stride=16), :] * ratio)
-            for k in range(2):
-                half = jnp.sum(jnp.where(low if k == 0 else ~low, product, 0.0), axis=1, keepdims=True)
-                row = jnp.sum(jnp.where(diagonal, half, 0.0), axis=0, keepdims=True)
-                own = jnp.where(sub == 2 * (2 * t + k) + m, row * scale, own)
-    for h in range(HEADS):
-        value = (nx[pl.ds(8 * (h // 2) + 2 + h % 2, 8, stride=16), :] * ratio).astype(BF16).astype(F32)
-        for m in range(2):
-            nv[pl.ds(2 * h + m, 8, stride=8), :] = value
+        acc = jnp.concatenate([acc[0:8, 0:128], acc[8:16, 128:256]], axis=0)
+        if t + 1 == ROWS // 2:
+            acc = acc + own_weight * own_value
+        place = pl.ds(pl.multiple_of(slot + 16 * order[t], 16), 16)
+        cx[place, :] = acc.astype(BF16)
+        spread(3, lambda p: cx.at[place, :], cx.at[place, :])
+
     for copy in late_loads[:3]:
         copy.wait()
     second = jnp.zeros((8, 1), F32)
     for h in range(HEADS):
         second = jnp.where(sub[:, :1] == 2 * h, hsw[0:1, h : h + 1], second)
-
-    everything(2, sx)
-    stats = [sx[s] for s in range(KV)]
-    peak = own
-    for s in stats:
-        peak = jnp.maximum(peak, s)
-    own_weight = jnp.exp(own - peak)
-    factors = [jnp.exp(s - peak) for s in stats]
-    weight_sum = own_weight
-    for f, s in zip(factors, stats):
-        weight_sum = weight_sum + f * pltpu.roll(s, 120, 1)
-    inverse = 1.0 / weight_sum
-    everything(3, cx)
-    for b in range(0, ROWS, 2):
-        acc = [own_weight[:, b + k : b + k + 1] * nv[8 * (b + k) : 8 * (b + k) + 8, :] for k in range(2)]
-        for s in range(KV):
-            part = cx[s, 8 * b : 8 * b + 16, :].astype(F32)
-            for k in range(2):
-                acc[k] = acc[k] + factors[s][:, b + k : b + k + 1] * part[8 * k : 8 * k + 8]
-        for k in range(2):
-            averaged = acc[k] * inverse[:, b + k : b + k + 1]
-            difference = averaged - second * pltpu.roll(averaged, 7, 0)
-            norm = lax.rsqrt(jnp.mean(difference * difference, axis=1, keepdims=True) + HEAD_EPSILON)
-            df[8 * (b + k) : 8 * (b + k) + 8, :] = difference * norm * hg[...] * HEAD_SCALE
+    gain = hg[...] * HEAD_SCALE
+    square_mask = lax.rem(lax.broadcasted_iota(jnp.int32, (64, 128), 1), 64) == lax.broadcasted_iota(
+        jnp.int32, (64, 128), 0
+    )
+
+    everything(2, sx.at[0 : KV - 1, :])
+    stats = sx[...]
+    factors = jnp.exp(stats - jnp.max(stats, axis=0, keepdims=True))
+    weight_sum = jnp.sum(factors * pltpu.roll(stats, 64, 1), axis=0, keepdims=True)
+    factors = factors * (1.0 / weight_sum)
+    factors = jnp.where(low, factors[0:8], pltpu.roll(factors[8:16], DH, 1))
+    high = factors.astype(BF16).astype(F32)
+    mixing = jnp.concatenate(
+        [
+            jnp.concatenate(
+                [jnp.where(square_mask, part[j : j + 1], 0.0).astype(BF16) for j in range(KV // 2)], axis=1
+            )
+            for part in (high, factors - high)
+        ],
+        axis=0,
+    )
+    everything(3, cx.at[0 : 64 * (KV - 1), :])
+    both = jnp.dot(mixing, cx[...], preferred_element_type=F32)
+    averaged = both[0:64] + both[64:128]
+    for b in range(ROWS):
+        one = averaged[8 * b : 8 * b + 8]
+        difference = one - second * pltpu.roll(one, 7, 0)
+        norm = lax.rsqrt(jnp.mean(difference * difference, axis=1, keepdims=True) + HEAD_EPSILON)
+        df[8 * b : 8 * b + 8, :] = difference * norm * gain
     attended = jnp.concatenate([df[pl.ds(2 * h, 8, stride=8), :].astype(BF16) for h in range(HEADS)], axis=1)
     os_own[...] = jnp.dot(attended, ow_w[...], preferred_element_type=F32).astype(BF16)
     swap = pair(3, os_own, os_far)
@@ -295,21 +329,25 @@
         for t in range(FT):
             row = (t // HT) * GR + w * HT + t % HT
             gs[pl.ds(row, 8, stride=2 * GR), :] = part[:, 128 * t : 128 * t + 128]
+    high = square.astype(BF16).astype(F32)
     for half in range(2):
-        gs[pl.ds(half * GR + 2 * HT, 8, stride=2 * GR), :] = square
-    gx[kv] = gs[pl.ds(pl.multiple_of(kv * GR, 8), GR), :]
-    spread(5, lambda p: gs.at[pl.ds(pl.multiple_of(p * GR, 8), GR), :], gx.at[kv])
-    everything(5, gx)
-    total = gx[0]
+        gs[pl.ds(half * GR + 2 * HT, 8, stride=2 * GR), :] = high
+        gs[pl.ds(half * GR + 2 * HT + 1, 8, stride=2 * GR), :] = square - high
+    for j in range(KV):
+        gb[j] = gs[j * GR : j * GR + GR, :].astype(BF16)
+    gx[kv] = gb[kv]
+    spread(5, lambda p: gb.at[p], gx.at[kv])
+    everything(5, gx.at[0 : KV - 1])
+    total = gx[0].astype(F32)
     for s in range(1, KV):
-        total = total + gx[s]
-    mixer_ratio = ratio_of(total[2 * HT : 2 * HT + 1])
+        total = total + gx[s].astype(F32)
+    mixer_ratio = ratio_of(total[2 * HT : 2 * HT + 1] + total[2 * HT + 1 : 2 * HT + 2])
     gate = total[:HT] * mixer_ratio
     up = total[HT : 2 * HT] * mixer_ratio
     hidden = gate / (1.0 + jnp.exp(-gate)) * up
     hx[kv, 0:HT, :] = hidden.astype(BF16)
     spread(6, lambda p: hx.at[kv], hx.at[kv])
-    everything(6, hx)
+    everything(6, hx.at[0 : KV - 1])
     for s in range(KV):
         hs[16 * s : 16 * s + 16, :] = hx[s].astype(F32)
     hidden = jnp.concatenate(
@@ -320,9 +358,12 @@
     swap.wait_recv()
     result = mixed + (ds_own[...].astype(F32) + ds_far[...].astype(F32))
     result = jnp.where(tp == 0, result, pltpu.roll(result, DH, 1))
-    out_ref[...] = result[:, :64].astype(BF16)
+    out_v[...] = result[:, :64].astype(BF16)
+    store = pltpu.make_async_copy(out_v, out_ref, load_sem.at[len(loads)])
+    store.start()
     for copy in sends + spreads:
         copy.wait_send()
+    store.wait()
 
 
 def shards(
@@ -336,7 +377,7 @@
         layer_kernel,
         out_shape=jax.ShapeDtypeStruct((ROWS, 64), BF16),
         in_specs=[any_space] * 17,
-        out_specs=pl.BlockSpec(memory_space=pltpu.VMEM),
+        out_specs=any_space,
         scratch_shapes=[
             vmem((ROWS, 64), BF16), vmem((ROWS, 64), BF16),
             vmem((1, 64), BF16), vmem((1, 64), BF16), vmem((1, 64), BF16), vmem((1, 64), BF16),
@@ -344,13 +385,14 @@
             vmem((128, 512), BF16), vmem((1, HEADS), F32), vmem((1, 128), F32), vmem((512, 128), BF16),
             vmem((128, FF), BF16), vmem((128, FF), BF16), vmem((FF, 128), BF16),
             vmem((ROWS, KEYS, 128), BF16), vmem((ROWS, KEYS, 128), BF16), vmem((8, 128), F32),
-            vmem((KV, QR, 128), F32), vmem((KV * 8, 128), F32), vmem((KV, 8, 128), F32), vmem((KV * 8, 128), F32),
-            vmem((KV, 64, 128), BF16), vmem((KV, 8, 128), F32),
-            vmem((KV * GR, 128), F32), vmem((KV, GR, 128), F32),
-            vmem((KV, 16, 128), BF16), vmem((KV * 16, 128), F32), vmem((64, 128), F32), vmem((64, 128), F32),
+            vmem((256, 256), BF16), vmem((ROWS // 2, 256, KEYS), BF16),
+            vmem((KV, QR, 128), F32), vmem((KV * 8, 128), F32), vmem((KV, 8, 128), F32),
+            vmem((KV * 64, 128), BF16), vmem((KV, 128), F32),
+            vmem((KV * GR, 128), F32), vmem((KV, GR, 128), BF16), vmem((KV, GR, 128), BF16),
+            vmem((KV, 16, 128), BF16), vmem((KV * 16, 128), F32), vmem((64, 128), F32),
             vmem((2, 16, KEYS), F32), vmem((64, 128), F32),
-            vmem((8, 128), BF16), vmem((8, 128), BF16), vmem((8, 128), BF16), vmem((8, 128), BF16),
-            dma((17,)), dma((5,)), dma((5,)), dma((7,)), dma((7,)),
+            vmem((8, 128), BF16), vmem((8, 128), BF16), vmem((8, 128), BF16), vmem((8, 128), BF16), vmem((ROWS, 64), BF16),
+            dma((18,)), dma((5,)), dma((5,)), dma((7,)), dma((7,)),
         ],
         compiler_params=pltpu.CompilerParams(
             collective_id=0, has_side_effects=True, vmem_limit_bytes=60 * 1024 * 1024

time: 41.3 us -> 37.2 us (0.901)
  Pallas kernels: 39.9 us -> 35.8 us
    pallas_call x1, Pallas kernels: 39.9 us -> 35.8 us  [shards(): pl.pallas_call(layer_kernel, out_shape=jax.ShapeDtypeStruct((ROWS, 64), B...]
where the time goes in v3:
time: 37.2 us; the launch traced here: 37.1 us
  Pallas kernels  35.8 us (96%)
  local copies, waits for them, and re-layouts  1.26 us (3%)
    pallas_call x1, Pallas kernels, shards(): pl.pallas_call(layer_kernel, out_shape=jax.ShapeDtypeStruct((ROWS, 64), B...  35.8 us
    unnamed x1, local copies, waits for them, and re-layouts  1.26 us

profile of v3, /device:TPU:1, one launch (start us, length us, event | category | flops | bytes accessed | tf_op | source)
XLA Modules:
  0.0 37.1 jit_solution(688303441653648259)
XLA Ops:
  0.0 35.8 %layer.1 = bf16[8,64]{1,0:T(8,128)(2,1)} custom-call(bf16[8,64]{1,0:T(8,128)(2,1)} %tok_h.1, bf16[1,64]{1,0:T(2,128)(2,1)} %bitcast.8, bf16[128,256]{1,0:T(8,128)(2,1)} %q1_h.1, bf16[128,256]{1,0:T(8,128)(2,1)} %q2_h.1, bf16[128,256]{1,0:T(8,128)(2,1)} %k1_h.1, bf16[128,256]{1,0:T(8,128)(2,1)} %k2_h.1, bf16[128,512]{1,0:T(8,128)(2,1)} %vw_h.1, ...), custom_call_target="tpu_custom_call" | custom-call | tf_op jit(solution)/shard_map/layer/pallas_call | solution.py:376
  35.8 1.3 %copy.19 = bf16[8,64]{1,0:T(8,128)(2,1)} copy(bf16[8,64]{1,0:T(8,128)(2,1)} %layer.1) | data formatting | bytes 2048

commit v4 on v3

--- a/solution.py
+++ b/solution.py
@@ -54,7 +54,7 @@
     out_ref,
     tok_own, tok_far, ag_own, ag_far, mg_own, mg_far,
     q1_w, q2_w, k1_w, k2_w, vw_w, hsw, hg, ow_w, gw_w, uw_w, dw_w, kc, vc, tab,
-    unit, kt, qx, rs, rx, cx, sx, gs, gb, gx, hx, hs, qs, sc, df, os_own, os_far, ds_own, ds_far, out_v,
+    unit, kt, qx, rs, rx, cx, sx, gs, gb, gx, hx, hs, qs, sc, df, os_own, os_far, dw_far, ds, out_v,
     load_sem, pair_send, pair_recv, all_send, all_recv,
 ):
     dp, kv, tp = (lax.axis_index(a) for a in ("dp", "kv", "tp"))
@@ -76,11 +76,12 @@
 
     first = [load(a, b) for a, b in ((tok_h, tok_own), (ag_h, ag_own), (mg_h, mg_own))]
     q_loads = [load(a, b) for a, b in ((q1_h, q1_w), (q2_h, q2_w), (tab_h, tab))]
+    down_load = load(dw_h, dw_w)
     kv_loads = [load(a, b) for a, b in ((k1_h, k1_w), (k2_h, k2_w), (vw_h, vw_w))]
     cache_loads = [load(kc_h, kc), load(vc_h, vc)]
     late_loads = [
         load(a, b)
-        for a, b in ((hsw_h, hsw), (hg_h, hg), (ow_h, ow_w), (gw_h, gw_w), (uw_h, uw_w), (dw_h, dw_w))
+        for a, b in ((hsw_h, hsw), (hg_h, hg), (ow_h, ow_w), (gw_h, gw_w), (uw_h, uw_w))
     ]
     for copy in first:
         copy.wait()
@@ -116,6 +117,8 @@
     diagonal = lane == sub
     for copy in q_loads:
         copy.wait()
+    down_load.wait()
+    swap_down = pair(4, dw_w, dw_far)
     for copy in swaps:
         copy.wait_recv()
 
@@ -345,18 +348,39 @@
     gate = total[:HT] * mixer_ratio
     up = total[HT : 2 * HT] * mixer_ratio
     hidden = gate / (1.0 + jnp.exp(-gate)) * up
-    hx[kv, 0:HT, :] = hidden.astype(BF16)
-    spread(6, lambda p: hx.at[kv], hx.at[kv])
-    everything(6, hx.at[0 : KV - 1])
-    for s in range(KV):
+    mine = hx.at[KV * tp + kv, 0 : HT + 1]
+    hx[KV * tp + kv, 0 : HT + 1, :] = jnp.concatenate([hidden, zero[0:1]], axis=0).astype(BF16)
+
+    def share(p, core):
+        pltpu.make_async_remote_copy(
+            mine, mine, all_send.at[6], all_recv.at[6], device_id=(dp, p, core), device_id_type=MESH
+        ).start()
+
+    for p in peers:
+        share(p, 1 - tp)
+        share(p, tp)
+    share(kv, 1 - tp)
+    swap_down.wait_recv()
+    everything(6, hx.at[0 : 2 * KV - 1, 0 : HT + 1])
+    for s in range(2 * KV):
         hs[16 * s : 16 * s + 16, :] = hx[s].astype(F32)
-    hidden = jnp.concatenate(
-        [hs[pl.ds(16 * (t // HT) + t % HT, 8, stride=32), :].astype(BF16) for t in range(FT)], axis=1
-    )
-    ds_own[...] = jnp.dot(hidden, dw_w[...], preferred_element_type=F32).astype(BF16)
-    swap = pair(4, ds_own, ds_far)
-    swap.wait_recv()
-    result = mixed + (ds_own[...].astype(F32) + ds_far[...].astype(F32))
+    result = zero
+    for core, weights in ((tp, dw_w), (1 - tp, dw_far)):
+        at = pl.multiple_of(16 * KV * core, 8)
+        hidden = jnp.concatenate(
+            [
+                jnp.concatenate([hs[pl.ds(at + 128 * k + t, 8, stride=16), :] for k in range(2)], axis=0).astype(BF16)
+                for t in range(HT)
+            ],
+            axis=1,
+        )
+        down = jnp.concatenate([weights[0 : FF // 2, :], weights[FF // 2 : FF, :]], axis=1)
+        part = jnp.dot(hidden, down, preferred_element_type=F32)
+        ds[0:16, :] = part[:, 0:128]
+        ds[16:32, :] = part[:, 128:256]
+        part = ds[pl.ds(0, 8, stride=2), :] + ds[pl.ds(17, 8, stride=2), :]
+        result = result + part.astype(BF16).astype(F32)
+    result = mixed + result
     result = jnp.where(tp == 0, result, pltpu.roll(result, DH, 1))
     out_v[...] = result[:, :64].astype(BF16)
     store = pltpu.make_async_copy(out_v, out_ref, load_sem.at[len(loads)])
@@ -389,9 +413,9 @@
             vmem((KV, QR, 128), F32), vmem((KV * 8, 128), F32), vmem((KV, 8, 128), F32),
             vmem((KV * 64, 128), BF16), vmem((KV, 128), F32),
             vmem((KV * GR, 128), F32), vmem((KV, GR, 128), BF16), vmem((KV, GR, 128), BF16),
-            vmem((KV, 16, 128), BF16), vmem((KV * 16, 128), F32), vmem((64, 128), F32),
+            vmem((2 * KV, 16, 128), BF16), vmem((2 * KV * 16, 128), F32), vmem((64, 128), F32),
             vmem((2, 16, KEYS), F32), vmem((64, 128), F32),
-            vmem((8, 128), BF16), vmem((8, 128), BF16), vmem((8, 128), BF16), vmem((8, 128), BF16), vmem((ROWS, 64), BF16),
+            vmem((8, 128), BF16), vmem((8, 128), BF16), vmem((FF, 128), BF16), vmem((32, 128), F32), vmem((ROWS, 64), BF16),
             dma((18,)), dma((5,)), dma((5,)), dma((7,)), dma((7,)),
         ],
         compiler_params=pltpu.CompilerParams(

time: 37.2 us -> 36.2 us (0.973)
  Pallas kernels: 35.8 us -> 34.8 us
    pallas_call x1, Pallas kernels: 35.8 us -> 34.8 us  [shards(): pl.pallas_call(layer_kernel, out_shape=jax.ShapeDtypeStruct((ROWS, 64), B...]
where the time goes in v4:
time: 36.2 us; the launch traced here: 36.1 us
  Pallas kernels  34.8 us (96%)
  local copies, waits for them, and re-layouts  1.26 us (3%)
    pallas_call x1, Pallas kernels, shards(): pl.pallas_call(layer_kernel, out_shape=jax.ShapeDtypeStruct((ROWS, 64), B...  34.8 us
    unnamed x1, local copies, waits for them, and re-layouts  1.26 us

profile of v4, /device:TPU:1, one launch (start us, length us, event | category | flops | bytes accessed | tf_op | source)
XLA Modules:
  0.0 36.1 jit_solution(2042273984863650447)
XLA Ops:
  0.0 34.8 %layer.1 = bf16[8,64]{1,0:T(8,128)(2,1)} custom-call(bf16[8,64]{1,0:T(8,128)(2,1)} %tok_h.1, bf16[1,64]{1,0:T(2,128)(2,1)} %bitcast.8, bf16[128,256]{1,0:T(8,128)(2,1)} %q1_h.1, bf16[128,256]{1,0:T(8,128)(2,1)} %q2_h.1, bf16[128,256]{1,0:T(8,128)(2,1)} %k1_h.1, bf16[128,256]{1,0:T(8,128)(2,1)} %k2_h.1, bf16[128,512]{1,0:T(8,128)(2,1)} %vw_h.1, ...), custom_call_target="tpu_custom_call" | custom-call | tf_op jit(solution)/shard_map/layer/pallas_call | solution.py:400
  34.8 1.3 %copy.19 = bf16[8,64]{1,0:T(8,128)(2,1)} copy(bf16[8,64]{1,0:T(8,128)(2,1)} %layer.1) | data formatting | bytes 2048

commit v5 on v4

--- a/solution.py
+++ b/solution.py
@@ -55,7 +55,7 @@
     tok_own, tok_far, ag_own, ag_far, mg_own, mg_far,
     q1_w, q2_w, k1_w, k2_w, vw_w, hsw, hg, ow_w, gw_w, uw_w, dw_w, kc, vc, tab,
     unit, kt, qx, rs, rx, cx, sx, gs, gb, gx, hx, hs, qs, sc, df, os_own, os_far, dw_far, ds, out_v,
-    load_sem, pair_send, pair_recv, all_send, all_recv,
+    ready, load_sem, pair_send, pair_recv, all_send, all_recv,
 ):
     dp, kv, tp = (lax.axis_index(a) for a in ("dp", "kv", "tp"))
     barrier = pltpu.get_barrier_semaphore()
@@ -63,7 +63,7 @@
     across, along = kv // 4, lax.rem(kv, 4)
     peers = [lax.rem(across + i, 4) * 4 + lax.rem(along + j, 4) for i, j in OFFSETS]
     for p in peers:
-        pl.semaphore_signal(barrier, 1, device_id=(dp, p, tp), device_id_type=MESH)
+        pl.semaphore_signal(barrier, 1, device_id=(dp, p, 1), device_id_type=MESH)
     pl.semaphore_signal(barrier, 1, device_id=partner, device_id_type=MESH)
 
     loads = []
@@ -83,9 +83,17 @@
         load(a, b)
         for a, b in ((hsw_h, hsw), (hg_h, hg), (ow_h, ow_w), (gw_h, gw_w), (uw_h, uw_w))
     ]
+    @pl.when(tp == 0)
+    def _():
+        pl.semaphore_wait(barrier, 1)
+        pl.semaphore_signal(ready.at[0], 1, device_id=partner, device_id_type=MESH)
+
+    @pl.when(tp == 1)
+    def _():
+        pl.semaphore_wait(ready.at[0], 1)
+
     for copy in first:
         copy.wait()
-    pl.semaphore_wait(barrier, KV)
 
     sends, spreads = [], []
 
@@ -136,8 +144,6 @@
         for t in range(2):
             qx[kv, 16 * w + 8 * t : 16 * w + 8 * t + 8, :] = part[:, 128 * t : 128 * t + 128]
     qx[kv, 32:33, :] = square_row
-    spread(0, lambda p: qx.at[kv], qx.at[kv])
-
     for copy in kv_loads:
         copy.wait()
     for w, ref in enumerate((k1_w, k2_w)):
@@ -147,6 +153,16 @@
     part = jnp.dot(scaled, vw_w[...], preferred_element_type=F32)
     for t in range(HEADS):
         rs[pl.ds(8 * (t // 2) + 2 + t % 2, 8, stride=16), :] = part[:, 128 * t : 128 * t + 128]
+    @pl.when(tp == 1)
+    def _():
+        pl.semaphore_wait(barrier, 2 * KV - 1)
+        pl.semaphore_signal(ready.at[1], 1, device_id=partner, device_id_type=MESH)
+
+    @pl.when(tp == 0)
+    def _():
+        pl.semaphore_wait(ready.at[1], 1)
+
+    spread(0, lambda p: qx.at[kv], qx.at[kv])
     rx[kv] = rs[pl.ds(pl.multiple_of(8 * kv, 8), 8), :]
     spread(1, lambda p: rs.at[pl.ds(pl.multiple_of(8 * p, 8), 4), :], rx.at[kv, 0:4])
 
@@ -416,7 +432,7 @@
             vmem((2 * KV, 16, 128), BF16), vmem((2 * KV * 16, 128), F32), vmem((64, 128), F32),
             vmem((2, 16, KEYS), F32), vmem((64, 128), F32),
             vmem((8, 128), BF16), vmem((8, 128), BF16), vmem((FF, 128), BF16), vmem((32, 128), F32), vmem((ROWS, 64), BF16),
-            dma((18,)), dma((5,)), dma((5,)), dma((7,)), dma((7,)),
+            pltpu.SemaphoreType.REGULAR((2,)), dma((18,)), dma((5,)), dma((5,)), dma((7,)), dma((7,)),
         ],
         compiler_params=pltpu.CompilerParams(
             collective_id=0, has_side_effects=True, vmem_limit_bytes=60 * 1024 * 1024

time: 36.2 us -> 35.6 us (0.983)
  Pallas kernels: 34.8 us -> 34.2 us
    pallas_call x1, Pallas kernels: 34.8 us -> 34.2 us  [shards(): pl.pallas_call(layer_kernel, out_shape=jax.ShapeDtypeStruct((ROWS, 64), B...]
where the time goes in v5:
time: 35.6 us; the launch traced here: 35.5 us
  Pallas kernels  34.2 us (96%)
  local copies, waits for them, and re-layouts  1.26 us (4%)
    pallas_call x1, Pallas kernels, shards(): pl.pallas_call(layer_kernel, out_shape=jax.ShapeDtypeStruct((ROWS, 64), B...  34.2 us
    unnamed x1, local copies, waits for them, and re-layouts  1.26 us

profile of v5, /device:TPU:1, one launch (start us, length us, event | category | flops | bytes accessed | tf_op | source)
XLA Modules:
  0.0 35.5 jit_solution(3355117730771298102)
XLA Ops:
  0.0 34.2 %layer.1 = bf16[8,64]{1,0:T(8,128)(2,1)} custom-call(bf16[8,64]{1,0:T(8,128)(2,1)} %tok_h.1, bf16[1,64]{1,0:T(2,128)(2,1)} %bitcast.8, bf16[128,256]{1,0:T(8,128)(2,1)} %q1_h.1, bf16[128,256]{1,0:T(8,128)(2,1)} %q2_h.1, bf16[128,256]{1,0:T(8,128)(2,1)} %k1_h.1, bf16[128,256]{1,0:T(8,128)(2,1)} %k2_h.1, bf16[128,512]{1,0:T(8,128)(2,1)} %vw_h.1, ...), custom_call_target="tpu_custom_call" | custom-call | tf_op jit(solution)/shard_map/layer/pallas_call | solution.py:416
  34.2 1.3 %copy.19 = bf16[8,64]{1,0:T(8,128)(2,1)} copy(bf16[8,64]{1,0:T(8,128)(2,1)} %layer.1) | data formatting | bytes 2048

commit v6 on v5

--- a/solution.py
+++ b/solution.py
@@ -26,7 +26,7 @@
 FLOOR = -1e30
 LOG2E = 1.4426950408889634
 KEYS = POSITIONS * HEADS
-QR = 33
+QR = 34
 GR = 24
 
 
@@ -142,8 +142,9 @@
     for w, ref in enumerate((q1_w, q2_w)):
         part = jnp.dot(scaled, ref[...], preferred_element_type=F32)
         for t in range(2):
-            qx[kv, 16 * w + 8 * t : 16 * w + 8 * t + 8, :] = part[:, 128 * t : 128 * t + 128]
-    qx[kv, 32:33, :] = square_row
+            qx[kv, 16 * w + 8 * t : 16 * w + 8 * t + 8, :] = part[:, 128 * t : 128 * t + 128].astype(BF16)
+    high = square_row.astype(BF16).astype(F32)
+    qx[kv, 32:34, :] = jnp.concatenate([high, square_row - high], axis=0).astype(BF16)
     for copy in kv_loads:
         copy.wait()
     for w, ref in enumerate((k1_w, k2_w)):
@@ -185,9 +186,10 @@
     def ratio_of(total):
         return lax.rsqrt(total / D + NORM_EPSILON)
 
-    square_total = qx[0, 32:33, :]
+    square_total = qx[0, 32:34, :].astype(F32)
     for s in range(1, KV):
-        square_total = square_total + qx[s, 32:33, :]
+        square_total = square_total + qx[s, 32:34, :].astype(F32)
+    square_total = jnp.sum(square_total, axis=0, keepdims=True)
     ratio_row = ratio_of(square_total)
     ratio = jnp.sum(jnp.where(diagonal, ratio_row, 0.0), axis=1, keepdims=True)
     cosine, sine = tab[0:1, :], tab[1:2, :]
@@ -198,9 +200,9 @@
         return (x * cosine + turned * sine).astype(BF16).astype(F32)
 
     def total_of(ref, at):
-        total = ref[0, at : at + 8, :]
+        total = ref[0, at : at + 8, :].astype(F32)
         for s in range(1, KV):
-            total = total + ref[s, at : at + 8, :]
+            total = total + ref[s, at : at + 8, :].astype(F32)
         return total
 
     query = [[rotated(total_of(qx, 16 * m + 8 * t) * ratio) for t in range(2)] for m in range(2)]
@@ -398,12 +400,9 @@
         result = result + part.astype(BF16).astype(F32)
     result = mixed + result
     result = jnp.where(tp == 0, result, pltpu.roll(result, DH, 1))
-    out_v[...] = result[:, :64].astype(BF16)
-    store = pltpu.make_async_copy(out_v, out_ref, load_sem.at[len(loads)])
-    store.start()
+    out_ref[...] = result[:, :64].astype(BF16)
     for copy in sends + spreads:
         copy.wait_send()
-    store.wait()
 
 
 def shards(
@@ -415,9 +414,9 @@
     dma = pltpu.SemaphoreType.DMA
     return pl.pallas_call(
         layer_kernel,
-        out_shape=jax.ShapeDtypeStruct((ROWS, 64), BF16),
+        out_shape=pltpu.VMEM((ROWS, 64), BF16),
         in_specs=[any_space] * 17,
-        out_specs=any_space,
+        out_specs=pl.BlockSpec(memory_space=pltpu.VMEM),
         scratch_shapes=[
             vmem((ROWS, 64), BF16), vmem((ROWS, 64), BF16),
             vmem((1, 64), BF16), vmem((1, 64), BF16), vmem((1, 64), BF16), vmem((1, 64), BF16),
@@ -426,7 +425,7 @@
             vmem((128, FF), BF16), vmem((128, FF), BF16), vmem((FF, 128), BF16),
             vmem((ROWS, KEYS, 128), BF16), vmem((ROWS, KEYS, 128), BF16), vmem((8, 128), F32),
             vmem((256, 256), BF16), vmem((ROWS // 2, 256, KEYS), BF16),
-            vmem((KV, QR, 128), F32), vmem((KV * 8, 128), F32), vmem((KV, 8, 128), F32),
+            vmem((KV, QR, 128), BF16), vmem((KV * 8, 128), F32), vmem((KV, 8, 128), F32),
             vmem((KV * 64, 128), BF16), vmem((KV, 128), F32),
             vmem((KV * GR, 128), F32), vmem((KV, GR, 128), BF16), vmem((KV, GR, 128), BF16),
             vmem((2 * KV, 16, 128), BF16), vmem((2 * KV * 16, 128), F32), vmem((64, 128), F32),

time: 35.6 us -> 33.3 us (0.935)
  Pallas kernels: 34.2 us -> 32.7 us
  local copies, waits for them, and re-layouts: 1.26 us -> 0.58 us
    pallas_call x1, Pallas kernels: 34.2 us -> 32.7 us  [shards(): pl.pallas_call(layer_kernel, out_shape=pltpu.VMEM((ROWS, 64), BF16), in_s...]
    unnamed x1, local copies, waits for them, and re-layouts: 1.26 us -> 0.58 us
where the time goes in v6:
time: 33.3 us; the launch traced here: 33.2 us
  Pallas kernels  32.7 us (98%)
  local copies, waits for them, and re-layouts  0.58 us (2%)
    pallas_call x1, Pallas kernels, shards(): pl.pallas_call(layer_kernel, out_shape=pltpu.VMEM((ROWS, 64), BF16), in_s...  32.7 us

profile of v6, /device:TPU:1, one launch (start us, length us, event | category | flops | bytes accessed | tf_op | source)
XLA Modules:
  0.0 33.2 jit_solution(17456441256379005726)
XLA Ops:
  0.0 32.7 %layer.1 = bf16[8,64]{1,0:T(8,128)(2,1)S(1)} custom-call(bf16[8,64]{1,0:T(8,128)(2,1)} %tok_h.1, bf16[1,64]{1,0:T(2,128)(2,1)} %bitcast.8, bf16[128,256]{1,0:T(8,128)(2,1)} %q1_h.1, bf16[128,256]{1,0:T(8,128)(2,1)} %q2_h.1, bf16[128,256]{1,0:T(8,128)(2,1)} %k1_h.1, bf16[128,256]{1,0:T(8,128)(2,1)} %k2_h.1, bf16[128,512]{1,0:T(8,128)(2,1)} %vw_h.1, ...), custom_call_target="tpu_custom_call" | custom-call | tf_op jit(solution)/shard_map/layer/pallas_call | solution.py:415
  32.7 0.6 %copy.19 = bf16[8,64]{1,0:T(8,128)(2,1)} copy(bf16[8,64]{1,0:T(8,128)(2,1)S(1)} %layer.1) | data formatting | bytes 2048

commit v7 on v5

--- a/solution.py
+++ b/solution.py
@@ -30,9 +30,8 @@
 GR = 24
 
 
-OFFSETS = sorted(
-    ((i, j) for i in range(4) for j in range(4) if (i, j) != (0, 0)),
-    key=lambda o: -min(o[0], 4 - o[0]) - min(o[1], 4 - o[1]),
+OFFSETS = (
+    (2, 2), (3, 2), (2, 3), (1, 2), (2, 1), (3, 3), (3, 1), (1, 3), (1, 1), (0, 2), (2, 0), (0, 3), (3, 0), (0, 1), (1, 0),
 )
 
 
@@ -54,7 +53,7 @@
     out_ref,
     tok_own, tok_far, ag_own, ag_far, mg_own, mg_far,
     q1_w, q2_w, k1_w, k2_w, vw_w, hsw, hg, ow_w, gw_w, uw_w, dw_w, kc, vc, tab,
-    unit, kt, qx, rs, rx, cx, sx, gs, gb, gx, hx, hs, qs, sc, df, os_own, os_far, dw_far, ds, out_v,
+    unit, kt, qx, rs, rx, cx, sx, gs, gb, gx, hx, hs, qs, sc, df, os_own, os_far, dw_far, ds,
     ready, load_sem, pair_send, pair_recv, all_send, all_recv,
 ):
     dp, kv, tp = (lax.axis_index(a) for a in ("dp", "kv", "tp"))
@@ -398,12 +397,9 @@
         result = result + part.astype(BF16).astype(F32)
     result = mixed + result
     result = jnp.where(tp == 0, result, pltpu.roll(result, DH, 1))
-    out_v[...] = result[:, :64].astype(BF16)
-    store = pltpu.make_async_copy(out_v, out_ref, load_sem.at[len(loads)])
-    store.start()
+    out_ref[...] = result[:, :64].astype(BF16)
     for copy in sends + spreads:
         copy.wait_send()
-    store.wait()
 
 
 def shards(
@@ -415,9 +411,9 @@
     dma = pltpu.SemaphoreType.DMA
     return pl.pallas_call(
         layer_kernel,
-        out_shape=jax.ShapeDtypeStruct((ROWS, 64), BF16),
+        out_shape=pltpu.VMEM((ROWS, 64), BF16),
         in_specs=[any_space] * 17,
-        out_specs=any_space,
+        out_specs=pl.BlockSpec(memory_space=pltpu.VMEM),
         scratch_shapes=[
             vmem((ROWS, 64), BF16), vmem((ROWS, 64), BF16),
             vmem((1, 64), BF16), vmem((1, 64), BF16), vmem((1, 64), BF16), vmem((1, 64), BF16),
@@ -431,8 +427,8 @@
             vmem((KV * GR, 128), F32), vmem((KV, GR, 128), BF16), vmem((KV, GR, 128), BF16),
             vmem((2 * KV, 16, 128), BF16), vmem((2 * KV * 16, 128), F32), vmem((64, 128), F32),
             vmem((2, 16, KEYS), F32), vmem((64, 128), F32),
-            vmem((8, 128), BF16), vmem((8, 128), BF16), vmem((FF, 128), BF16), vmem((32, 128), F32), vmem((ROWS, 64), BF16),
-            pltpu.SemaphoreType.REGULAR((2,)), dma((18,)), dma((5,)), dma((5,)), dma((7,)), dma((7,)),
+            vmem((8, 128), BF16), vmem((8, 128), BF16), vmem((FF, 128), BF16), vmem((32, 128), F32),
+            pltpu.SemaphoreType.REGULAR((2,)), dma((17,)), dma((5,)), dma((5,)), dma((7,)), dma((7,)),
         ],
         compiler_params=pltpu.CompilerParams(
             collective_id=0, has_side_effects=True, vmem_limit_bytes=60 * 1024 * 1024

time: 35.6 us -> 33.9 us (0.952)
  Pallas kernels: 34.2 us -> 33.2 us
  local copies, waits for them, and re-layouts: 1.26 us -> 0.58 us
    pallas_call x1, Pallas kernels: 34.2 us -> 33.2 us  [shards(): pl.pallas_call(layer_kernel, out_shape=pltpu.VMEM((ROWS, 64), BF16), in_s...]
    unnamed x1, local copies, waits for them, and re-layouts: 1.26 us -> 0.58 us
where the time goes in v7:
time: 33.9 us; the launch traced here: 33.8 us
  Pallas kernels  33.2 us (98%)
  local copies, waits for them, and re-layouts  0.58 us (2%)
    pallas_call x1, Pallas kernels, shards(): pl.pallas_call(layer_kernel, out_shape=pltpu.VMEM((ROWS, 64), BF16), in_s...  33.2 us

profile of v7, /device:TPU:1, one launch (start us, length us, event | category | flops | bytes accessed | tf_op | source)
XLA Modules:
  0.0 33.8 jit_solution(11616852046088319374)
XLA Ops:
  0.0 33.2 %layer.1 = bf16[8,64]{1,0:T(8,128)(2,1)S(1)} custom-call(bf16[8,64]{1,0:T(8,128)(2,1)} %tok_h.1, bf16[1,64]{1,0:T(2,128)(2,1)} %bitcast.8, bf16[128,256]{1,0:T(8,128)(2,1)} %q1_h.1, bf16[128,256]{1,0:T(8,128)(2,1)} %q2_h.1, bf16[128,256]{1,0:T(8,128)(2,1)} %k1_h.1, bf16[128,256]{1,0:T(8,128)(2,1)} %k2_h.1, bf16[128,512]{1,0:T(8,128)(2,1)} %vw_h.1, ...), custom_call_target="tpu_custom_call" | custom-call | tf_op jit(solution)/shard_map/layer/pallas_call | solution.py:412
  33.2 0.6 %copy.19 = bf16[8,64]{1,0:T(8,128)(2,1)} copy(bf16[8,64]{1,0:T(8,128)(2,1)S(1)} %layer.1) | data formatting | bytes 2048

commit v8 on v7

--- a/solution.py
+++ b/solution.py
@@ -163,7 +163,6 @@
 
     spread(0, lambda p: qx.at[kv], qx.at[kv])
     rx[kv] = rs[pl.ds(pl.multiple_of(8 * kv, 8), 8), :]
-    spread(1, lambda p: rs.at[pl.ds(pl.multiple_of(8 * p, 8), 4), :], rx.at[kv, 0:4])
 
     wide = (256, 256)
     unit[...] = (lax.broadcasted_iota(jnp.int32, wide, 0) == lax.broadcasted_iota(jnp.int32, wide, 1)).astype(BF16)
@@ -177,7 +176,9 @@
             kt[b // 2, :, pl.ds(at, 512)] = turned.astype(BF16)
         return carry
 
-    lax.fori_loop(0, KEYS // 512, turn, 0)
+    lax.fori_loop(0, KEYS // 1024, turn, 0)
+    spread(1, lambda p: rs.at[pl.ds(pl.multiple_of(8 * p, 8), 4), :], rx.at[kv, 0:4])
+    lax.fori_loop(KEYS // 1024, KEYS // 512, turn, 0)
     cache_loads[1].wait()
     everything(0, qx.at[0 : KV - 1])
 

time: 33.9 us -> 33.9 us (level)
  no operation moved by 1% of the time
where the time goes in v8:
time: 33.9 us; the launch traced here: 33.8 us
  Pallas kernels  33.2 us (98%)
  local copies, waits for them, and re-layouts  0.58 us (2%)
    pallas_call x1, Pallas kernels, shards(): pl.pallas_call(layer_kernel, out_shape=pltpu.VMEM((ROWS, 64), BF16), in_s...  33.2 us

profile of v8, /device:TPU:1, one launch (start us, length us, event | category | flops | bytes accessed | tf_op | source)
XLA Modules:
  0.0 33.8 jit_solution(14844828422656824087)
XLA Ops:
  0.0 33.2 %layer.1 = bf16[8,64]{1,0:T(8,128)(2,1)S(1)} custom-call(bf16[8,64]{1,0:T(8,128)(2,1)} %tok_h.1, bf16[1,64]{1,0:T(2,128)(2,1)} %bitcast.8, bf16[128,256]{1,0:T(8,128)(2,1)} %q1_h.1, bf16[128,256]{1,0:T(8,128)(2,1)} %q2_h.1, bf16[128,256]{1,0:T(8,128)(2,1)} %k1_h.1, bf16[128,256]{1,0:T(8,128)(2,1)} %k2_h.1, bf16[128,512]{1,0:T(8,128)(2,1)} %vw_h.1, ...), custom_call_target="tpu_custom_call" | custom-call | tf_op jit(solution)/shard_map/layer/pallas_call | solution.py:413
  33.3 0.6 %copy.19 = bf16[8,64]{1,0:T(8,128)(2,1)} copy(bf16[8,64]{1,0:T(8,128)(2,1)S(1)} %layer.1) | data formatting | bytes 2048
